TPU v7x, 32 devices: a whole 2x2x4 slice. The times are simulated.
32 devices in a mesh: ep: 8 (over z, x), tp: 4 (over y, core).
Axes of the slice: x: 2, y: 2, z: 4, core: 2. Of those that a mesh axis runs over, the one named last changes fastest.
Arguments:
- query_latent: bfloat16 [2048, 512], P(('ep', 'tp')), may hold values from -6 to 6
- key_latent: bfloat16 [2048, 256], P(('ep', 'tp')), may hold values from -6 to 6
- rotary_key: bfloat16 [2048, 32], P(('ep', 'tp')), may hold values from -140 to 140
- query_gain: float32 [512], replicated, may hold values from 0.1 to 1.9
- latent_gain: float32 [256], replicated, may hold values from 0.1 to 1.9
- query_content: bfloat16 [512, 512], replicated, may hold values from -0.625 to 0.625
- query_rotary: bfloat16 [512, 256], replicated, may hold values from -0.625 to 0.625
- key_content: bfloat16 [256, 512], replicated, may hold values from -0.375 to 0.375
- value_weight: bfloat16 [256, 512], replicated, may hold values from -0.375 to 0.375
- output_weight: bfloat16 [512, 2048], P('tp'), may hold values from -1 to 1
- expert_input: bfloat16 [2048, 2048], P(('ep', 'tp')), may hold values from -6 to 6
- norm_gain: float32 [2048], replicated, may hold values from 0.1 to 1.9
- routes: int32 [2048, 2], P(('ep', 'tp')), may hold values from 0 to 15, all different within a row; in each aligned block of 64 rows (0 to 63, 64 to 127, ...) at most 16 rows name the same one
- route_weight: float32 [2048, 2], P(('ep', 'tp')), may hold values from 0.25 to 2
- expert_gate: bfloat16 [16, 2048, 1024], P('ep', None, 'tp'), may hold values from -0.125 to 0.125
- expert_up: bfloat16 [16, 2048, 1024], P('ep', None, 'tp'), may hold values from -0.125 to 0.125
- expert_down: bfloat16 [16, 1024, 2048], P('ep', 'tp'), may hold values from -0.1875 to 0.1875
- shared_gate: bfloat16 [2048, 1024], P(None, 'tp'), may hold values from -0.125 to 0.125
- shared_up: bfloat16 [2048, 1024], P(None, 'tp'), may hold values from -0.125 to 0.125
- shared_down: bfloat16 [1024, 2048], P('tp'), may hold values from -0.1875 to 0.1875
Outputs:
- mixer_out: bfloat16 [2048, 2048], P(('ep', 'tp'))
- expert_out: bfloat16 [2048, 2048], P(('ep', 'tp'))
Inputs may be any that keep to these rules, and one draw needn't show every extreme that they name: `routes`: each row names 2 different experts. Within the rows of one device (aligned blocks of 64 rows) no expert is named by more than 16 rows, and in every draw some expert is named by exactly 16 rows of some device.
All inputs are finite; a program needn't handle non-finite values.
Results may differ from a plain program's by a relative error of at most 0.013.
The roundings to bfloat16 on the way count: a program that leaves them out, or rounds other values in their place, can miss the bound.
Values may be sent and summed in bfloat16 or wider, within the bound.
A program may use at most 128 MiB of HBM per device.

v0:
```python
import math

import jax
import jax.numpy as jnp
from jax import lax
from jax.experimental import pallas as pl
from jax.experimental.pallas import tpu as pltpu
from jax.sharding import PartitionSpec as P

HEADS = 8
CONTENT = 64
ROTARY = 32
VALUE = 64


norm_eps = 1e-06
rope_base = 10000.0


def rms_rows(entries, gain_row):
    widened = entries.astype(jnp.float32)
    return widened * lax.rsqrt(jnp.mean(widened * widened, -1, keepdims=True) + norm_eps) * gain_row


def turn_pairs(entries, positions):
    width_full = entries.shape[-1]
    frequency = rope_base ** (-jnp.arange(width_full // 2, dtype=jnp.float32) * 2.0 / width_full)
    angles = positions.astype(jnp.float32)[:, None] * frequency[None, :]
    cosine = jnp.cos(angles)[:, None, :]
    sine_part = jnp.sin(angles)[:, None, :]
    even_part = entries[..., 0::2]
    odd_part = entries[..., 1::2]
    joined = jnp.stack(
        [even_part * cosine - odd_part * sine_part, even_part * sine_part + odd_part * cosine], -1
    )
    return joined.reshape(entries.shape)


def absorb_block(carried, query_part, query_turn, key_part, key_turn, value_rows, score_scale):
    running_peak, running_total, summed = carried
    scores = jnp.einsum("qhc,khc->qhk", query_part, key_part, preferred_element_type=jnp.float32)
    scores = scores + jnp.einsum(
        "qhr,kr->qhk", query_turn, key_turn, preferred_element_type=jnp.float32
    )
    scores = scores * score_scale
    new_peak = jnp.maximum(running_peak, jnp.max(scores, -1))
    factor = jnp.exp(running_peak - new_peak)
    weights = jnp.exp(scores - new_peak[..., None])
    running_total = running_total * factor + jnp.sum(weights, -1)
    summed = summed * factor[..., None] + jnp.einsum(
        "qhk,khv->qhv", weights.astype(jnp.bfloat16), value_rows, preferred_element_type=jnp.float32
    )
    return (new_peak, running_total, summed)


def absorb_piece(carried, query_part, query_turn, key_part, key_turn, value_rows, score_scale):
    row_count = key_part.shape[0]
    key_block = math.gcd(row_count, 2048)
    if key_block == row_count:
        return absorb_block(
            carried, query_part, query_turn, key_part, key_turn, value_rows, score_scale
        )
    block_count = row_count // key_block

    def advance(state, pieces):
        return (
            absorb_block(
                state, query_part, query_turn, pieces[0], pieces[1], pieces[2], score_scale
            ),
            None,
        )

    stacked = (
        key_part.reshape((block_count, key_block) + key_part.shape[1:]),
        key_turn.reshape(block_count, key_block, key_turn.shape[1]),
        value_rows.reshape((block_count, key_block) + value_rows.shape[1:]),
    )
    carried, ignored = lax.scan(advance, carried, stacked)
    return carried


def expand_keys(latent_rows, key_columns, value_columns, head_local):
    row_count = latent_rows.shape[0]
    key_part = (
        jnp.dot(latent_rows, key_columns, preferred_element_type=jnp.float32)
        .astype(jnp.bfloat16)
        .reshape(row_count, head_local, CONTENT)
    )
    value_rows = (
        jnp.dot(latent_rows, value_columns, preferred_element_type=jnp.float32)
        .astype(jnp.bfloat16)
        .reshape(row_count, head_local, VALUE)
    )
    return (key_part, value_rows)


def expert_terms(row_block, gate_weight, up_weight, down_weight):
    gated = jnp.einsum("secd,edf->secf", row_block, gate_weight, preferred_element_type=jnp.float32)
    lifted = jnp.einsum("secd,edf->secf", row_block, up_weight, preferred_element_type=jnp.float32)
    hidden = (jax.nn.silu(gated) * lifted).astype(jnp.bfloat16)
    return jnp.einsum("secf,efd->secd", hidden, down_weight, preferred_element_type=jnp.float32)


def shared_terms(row_block, gate_weight, up_weight, down_weight):
    gated = jnp.dot(row_block, gate_weight, preferred_element_type=jnp.float32)
    lifted = jnp.dot(row_block, up_weight, preferred_element_type=jnp.float32)
    hidden = (jax.nn.silu(gated) * lifted).astype(jnp.bfloat16)
    return jnp.dot(hidden, down_weight, preferred_element_type=jnp.float32)


def shards_plain(
    query_latent,
    key_latent,
    rotary_key,
    query_gain,
    latent_gain,
    query_content,
    query_rotary,
    key_content,
    value_weight,
    output_weight,
    expert_input,
    norm_gain,
    routes,
    route_weight,
    expert_gate,
    expert_up,
    expert_down,
    shared_gate,
    shared_up,
    shared_down,
):
    group_size = lax.axis_size("tp")
    expert_groups = lax.axis_size("ep")
    own_rows = query_latent.shape[0]
    head_local = HEADS // group_size
    head_index = lax.axis_index("tp")
    group_rows_count = own_rows * group_size
    group_start = lax.axis_index("ep") * group_rows_count
    own_start = group_start + head_index * own_rows
    score_scale = (CONTENT + ROTARY) ** (-0.5)
    query_normed = rms_rows(query_latent, query_gain).astype(jnp.bfloat16)
    latent_normed = rms_rows(key_latent, latent_gain).astype(jnp.bfloat16)
    own_positions = own_start + jnp.arange(own_rows, dtype=jnp.int32)
    key_turned = turn_pairs(rotary_key.astype(jnp.float32)[:, None, :], own_positions)[
        :, 0, :
    ].astype(jnp.bfloat16)
    token_rows = expert_input.shape[0]
    picks = routes.shape[1]
    local_experts = expert_gate.shape[0]
    expert_total = local_experts * expert_groups
    capacity = 2 * token_rows * picks // expert_total
    slot_total = expert_total * capacity
    model_width = expert_input.shape[1]
    expert_normed = rms_rows(expert_input, norm_gain).astype(jnp.bfloat16)
    flat_routes = routes.reshape(-1)
    marks = (flat_routes[:, None] == jnp.arange(expert_total, dtype=jnp.int32)[None, :]).astype(
        jnp.int32
    )
    ranks = jnp.sum((jnp.cumsum(marks, 0) - marks) * marks, 1)
    targets = flat_routes * capacity + ranks
    picker = (jnp.arange(slot_total, dtype=jnp.int32)[:, None] == targets[None, :]).astype(
        jnp.int32
    )
    picker = jnp.sum(picker.reshape(slot_total, token_rows, picks), 2).astype(jnp.bfloat16)
    outgoing = jnp.dot(picker, expert_normed, preferred_element_type=jnp.float32).astype(
        jnp.bfloat16
    )
    outgoing = outgoing.reshape(expert_groups, local_experts, capacity, model_width)
    received = lax.all_to_all(outgoing, "ep", split_axis=0, concat_axis=0, tiled=True)
    group_query, group_latent, group_turn, gathered_rows, gathered_tokens = (
        lax.all_gather(query_normed, "tp", axis=0, tiled=True),
        lax.all_gather(latent_normed, "tp", axis=0, tiled=True),
        lax.all_gather(key_turned, "tp", axis=0, tiled=True),
        lax.all_gather(received, "tp", axis=0, tiled=True),
        lax.all_gather(expert_normed, "tp", axis=0, tiled=True),
    )
    positions = group_start + jnp.arange(group_rows_count, dtype=jnp.int32)
    content_columns = lax.dynamic_slice_in_dim(
        query_content, head_index * head_local * CONTENT, head_local * CONTENT, 1
    )
    rotary_columns = lax.dynamic_slice_in_dim(
        query_rotary, head_index * head_local * ROTARY, head_local * ROTARY, 1
    )
    query_part = (
        jnp.dot(group_query, content_columns, preferred_element_type=jnp.float32)
        .astype(jnp.bfloat16)
        .reshape(group_rows_count, head_local, CONTENT)
    )
    query_turn = turn_pairs(
        jnp.dot(group_query, rotary_columns, preferred_element_type=jnp.float32).reshape(
            group_rows_count, head_local, ROTARY
        ),
        positions,
    ).astype(jnp.bfloat16)
    key_columns = lax.dynamic_slice_in_dim(
        key_content, head_index * head_local * CONTENT, head_local * CONTENT, 1
    )
    value_columns = lax.dynamic_slice_in_dim(
        value_weight, head_index * head_local * VALUE, head_local * VALUE, 1
    )
    carry_start = (
        jnp.full((group_rows_count, head_local), -jnp.inf, jnp.float32),
        jnp.zeros((group_rows_count, head_local), jnp.float32),
        jnp.zeros((group_rows_count, head_local, VALUE), jnp.float32),
    )
    key_part, value_rows = expand_keys(
        lax.all_gather(group_latent, "ep", axis=0, tiled=True),
        key_columns,
        value_columns,
        head_local,
    )
    running_peak, running_total, summed = absorb_piece(
        carry_start,
        query_part,
        query_turn,
        key_part,
        lax.all_gather(group_turn, "ep", axis=0, tiled=True),
        value_rows,
        score_scale,
    )
    attended = (
        (summed / running_total[..., None])
        .astype(jnp.bfloat16)
        .reshape(group_rows_count, head_local * VALUE)
    )
    routed_term = expert_terms(gathered_rows, expert_gate, expert_up, expert_down)
    shared_term = shared_terms(gathered_tokens, shared_gate, shared_up, shared_down)
    mixer_term = jnp.dot(attended, output_weight, preferred_element_type=jnp.float32)
    mixer_sum, routed_sum, shared_sum = (
        lax.psum_scatter(
            mixer_term.astype(jnp.bfloat16), "tp", scatter_dimension=0, tiled=True
        ).astype(jnp.float32),
        lax.psum_scatter(
            routed_term.astype(jnp.bfloat16), "tp", scatter_dimension=0, tiled=True
        ).astype(jnp.float32),
        lax.psum_scatter(
            shared_term.astype(jnp.bfloat16), "tp", scatter_dimension=0, tiled=True
        ).astype(jnp.float32),
    )
    mixer_out = mixer_sum.astype(jnp.bfloat16)
    returned = lax.all_to_all(
        routed_sum.astype(jnp.bfloat16), "ep", split_axis=0, concat_axis=0, tiled=True
    )
    returned = returned.reshape(slot_total, model_width)
    picked = jnp.take(returned, targets, axis=0).reshape(token_rows, picks, model_width)
    combined = jnp.sum(route_weight[..., None] * picked.astype(jnp.float32), 1) + shared_sum
    expert_out = combined.astype(jnp.bfloat16)
    return (mixer_out, expert_out)


MESH = pl.DeviceIdType.MESH
VMEM_LIMIT = 60 * 1024 * 1024


def greet(ep_count, me, head_index):
    barrier = pltpu.get_barrier_semaphore()
    for step in range(1, ep_count):
        pl.semaphore_signal(
            barrier, inc=1, device_id=(lax.rem(me + step, ep_count), head_index), device_id_type=MESH
        )
    row, core = head_index // 2, head_index % 2
    for other in ((1 - row) * 2 + core, row * 2 + 1 - core):
        pl.semaphore_signal(barrier, inc=1, device_id=(me, other), device_id_type=MESH)
    pl.semaphore_wait(barrier, ep_count + 1)


def gated_rows(rows, gate_weight, up_weight):
    gated = jnp.dot(rows, gate_weight, preferred_element_type=jnp.float32)
    lifted = jnp.dot(rows, up_weight, preferred_element_type=jnp.float32)
    return (gated / (1.0 + jnp.exp(-gated)) * lifted).astype(jnp.bfloat16)


def block_kernel(
    ep_count,
    capacity,
    query_latent_ref,
    key_latent_ref,
    rotary_key_ref,
    query_gain_ref,
    latent_gain_ref,
    expert_input_ref,
    norm_gain_ref,
    routes_ref,
    route_weight_ref,
    cosine_ref,
    sine_ref,
    query_content_hbm,
    query_rotary_hbm,
    key_content_hbm,
    value_weight_hbm,
    output_weight_hbm,
    gate_hbm,
    up_hbm,
    down_hbm,
    shared_gate_hbm,
    shared_up_hbm,
    shared_down_hbm,
    both_out,
    slots_ref,
    query_columns_ref,
    latent_columns_ref,
    output_weight_ref,
    weight_ref,
    rows,
    latents,
    tokens,
    queries,
    gate_ref,
    up_ref,
    down_ref,
    shared_gate_ref,
    shared_up_ref,
    shared_down_ref,
    keys,
    values,
    query_wide,
    attended,
    part,
    side,
    half_rows,
    half_side,
    far_rows,
    far_side,
    returned,
    ep_send,
    ep_recv,
    y_send,
    y_recv,
    core_send,
    core_recv,
    cross_send,
    cross_recv,
    own_sem,
    weight_sem,
    half_send,
    half_recv,
    far_send,
    far_recv,
    back_send,
    back_recv,
):
    me = lax.axis_index("ep")
    head_index = lax.axis_index("tp")
    row, core = head_index // 2, head_index % 2
    y_peer = (me, (1 - row) * 2 + core)
    core_peer = (me, row * 2 + 1 - core)
    local_experts = gate_ref.shape[0]
    width = rows.shape[-1]
    own_rows = tokens.shape[2]
    slot_rows = rows.shape[3]
    stripe = math.gcd(width, 512)

    def remote(source, target, send_sem, recv_sem, device):
        return pltpu.make_async_remote_copy(
            src_ref=source,
            dst_ref=target,
            send_sem=send_sem,
            recv_sem=recv_sem,
            device_id=device,
            device_id_type=MESH,
        )

    head_lanes = attended.shape[1]
    heads = head_lanes // VALUE
    columns = pl.ds(pl.multiple_of(head_index * head_lanes, head_lanes), head_lanes)
    turn_columns = pl.ds(pl.multiple_of(head_index * heads * ROTARY // 128 * 128, 128), 128)
    fetches = [
        pltpu.make_async_copy(source, target, weight_sem.at[place])
        for place, (source, target) in enumerate(
            (
                (query_content_hbm.at[:, columns], query_columns_ref.at[:, :head_lanes]),
                (query_rotary_hbm.at[:, turn_columns], query_columns_ref.at[:, head_lanes:]),
                (key_content_hbm.at[:, columns], latent_columns_ref.at[:, :head_lanes]),
                (value_weight_hbm.at[:, columns], latent_columns_ref.at[:, head_lanes:]),
                (output_weight_hbm, output_weight_ref),
                (shared_gate_hbm, shared_gate_ref),
                (shared_up_hbm, shared_up_ref),
                (shared_down_hbm, shared_down_ref),
                (gate_hbm, gate_ref),
                (up_hbm, up_ref),
                (down_hbm, down_ref),
            )
        )
    ]
    for fetch in fetches:
        fetch.start()

    def turn(entries, cosine, sine):
        lane = lax.broadcasted_iota(jnp.int32, entries.shape, 1)
        crossed = jnp.where(
            lane % 2 == 0, -pltpu.roll(entries, 127, 1), pltpu.roll(entries, 1, 1)
        )
        return (entries * cosine + crossed * sine).astype(jnp.bfloat16)

    latents[row, core, 0, :, : key_latent_ref.shape[1]] = rms_rows(
        key_latent_ref[...], latent_gain_ref[...]
    ).astype(jnp.bfloat16)
    repeats = jnp.where(
        lax.broadcasted_iota(jnp.int32, (ROTARY, 128), 0)
        == lax.broadcasted_iota(jnp.int32, (ROTARY, 128), 1) % ROTARY,
        1.0,
        0.0,
    ).astype(jnp.bfloat16)
    own_span = pl.ds(pl.multiple_of(head_index * own_rows, own_rows), own_rows)
    latents[row, core, 0, :, key_latent_ref.shape[1] :] = turn(
        lax.dot_general(
            rotary_key_ref[...],
            repeats,
            (((0,), (0,)), ((), ())),
            preferred_element_type=jnp.float32,
        ),
        cosine_ref[own_span, :],
        sine_ref[own_span, :],
    )
    queries[row, core] = rms_rows(query_latent_ref[...], query_gain_ref[...]).astype(jnp.bfloat16)
    greet(ep_count, me, head_index)

    def latent_ep(step):
        return remote(
            latents.at[row, core, 0],
            latents.at[row, core, step],
            ep_send.at[1, step],
            ep_recv.at[1, step],
            (lax.rem(me + step, ep_count), head_index),
        )

    def slots_ep(step):
        peer = lax.rem(me + step, ep_count)
        return remote(
            slots_ref.at[peer],
            rows.at[row, core, step],
            ep_send.at[0, step],
            ep_recv.at[0, step],
            (peer, head_index),
        )

    routes_of = {
        "y": (row, y_send, y_recv, y_peer),
        "core": (row, core_send, core_recv, core_peer),
        "cross": (1 - row, cross_send, cross_recv, core_peer),
    }

    def moved(buffer, place, step, route):
        origin_row, send_sem, recv_sem, device = routes_of[route]
        block = buffer.at[origin_row, core] if step == ep_count else buffer.at[origin_row, core, step]
        return remote(block, block, send_sem.at[place, step], recv_sem.at[place, step], device)

    for step in range(1, ep_count):
        latent_ep(step).start()
    for route in ("y", "core"):
        moved(queries, 1, ep_count, route).start()
        moved(latents, 1, 0, route).start()
    expert_normed = rms_rows(expert_input_ref[...], norm_gain_ref[...]).astype(jnp.bfloat16)
    tokens[row, core] = expert_normed
    for route in ("y", "core"):
        moved(tokens, 0, ep_count, route).start()
    expert_total = local_experts * ep_count
    expert_lane = lax.broadcasted_iota(jnp.int32, (own_rows, expert_total), 1)
    route_columns = routes_ref[...].T
    weight_columns = route_weight_ref[...].T
    named = [
        jnp.where(route_columns[:, pick : pick + 1] == expert_lane, 1.0, 0.0)
        for pick in range(routes_ref.shape[0])
    ]
    earlier = jnp.where(
        lax.broadcasted_iota(jnp.int32, (own_rows, own_rows), 0)
        > lax.broadcasted_iota(jnp.int32, (own_rows, own_rows), 1),
        1.0,
        0.0,
    ).astype(jnp.bfloat16)
    ahead = jnp.dot(earlier, sum(named).astype(jnp.bfloat16), preferred_element_type=jnp.float32)
    slot_lane = lax.broadcasted_iota(jnp.int32, (own_rows, ep_count * slot_rows), 1)
    picker = jnp.zeros(slot_lane.shape, jnp.float32)
    weight = jnp.zeros(slot_lane.shape, jnp.float32)
    for pick, marks in enumerate(named):
        rank = jnp.sum(ahead * marks, 1, keepdims=True).astype(jnp.int32)
        chosen = slot_lane == route_columns[:, pick : pick + 1] * capacity + rank
        picker = jnp.where(chosen, 1.0, picker)
        weight = jnp.where(chosen, weight_columns[:, pick : pick + 1], weight)
    high = weight.astype(jnp.bfloat16)
    rest = weight - high.astype(jnp.float32)
    middle = rest.astype(jnp.bfloat16)
    weight_ref[:own_rows] = high
    weight_ref[own_rows : 2 * own_rows] = middle
    weight_ref[2 * own_rows :] = (rest - middle.astype(jnp.float32)).astype(jnp.bfloat16)
    picker = picker.T.astype(jnp.bfloat16)
    for start in range(0, width, stripe):
        slots_ref[:, :, start : start + stripe] = (
            jnp.dot(
                picker, expert_normed[:, start : start + stripe], preferred_element_type=jnp.float32
            )
            .astype(jnp.bfloat16)
            .reshape(ep_count, slot_rows, stripe)
        )
    for step in range(1, ep_count):
        slots_ep(step).start()
    own_slots = pltpu.make_async_copy(slots_ref.at[me], rows.at[row, core, 0], own_sem.at[0])
    own_slots.start()
    own_slots.wait()
    for route in ("y", "core"):
        moved(rows, 0, 0, route).start()
    for step in range(1, ep_count):
        latent_ep(step).wait_recv()
        for route in ("y", "core"):
            moved(latents, 1, step, route).start()
    moved(queries, 1, ep_count, "y").wait_recv()
    moved(queries, 1, ep_count, "cross").start()
    moved(tokens, 0, ep_count, "y").wait_recv()
    moved(tokens, 0, ep_count, "cross").start()
    for step in range(ep_count):
        moved(latents, 1, step, "y").wait_recv()
        moved(latents, 1, step, "cross").start()
    for route in ("core", "cross"):
        moved(queries, 1, ep_count, route).wait_recv()
        for step in range(ep_count):
            moved(latents, 1, step, route).wait_recv()

    rank_width = latent_columns_ref.shape[0]
    group_rows = attended.shape[0]

    def project():
        for fetch in fetches[:5]:
            fetch.wait()
        query_rows = queries[...].reshape(group_rows, queries.shape[-1])
        projected = jnp.dot(
            query_rows, query_columns_ref[...], preferred_element_type=jnp.float32
        )
        query_wide[:, :head_lanes] = projected[:, :head_lanes].astype(jnp.bfloat16)
        query_wide[:, head_lanes:] = turn(
            projected[:, head_lanes:], cosine_ref[...], sine_ref[...]
        )
        for block in range(4):
            packed = latents[block // 2, block % 2].reshape(ep_count * own_rows, latents.shape[-1])
            expanded = jnp.dot(
                packed[:, :rank_width],
                latent_columns_ref[...],
                preferred_element_type=jnp.float32,
            ).astype(jnp.bfloat16)
            span = slice(block * ep_count * own_rows, (block + 1) * ep_count * own_rows)
            keys[span, :head_lanes] = expanded[:, :head_lanes]
            keys[span, head_lanes:] = packed[:, rank_width:]
            values[span, :] = expanded[:, head_lanes:]

    def attend(block):
        block_rows = group_rows // 4
        span = slice(block * block_rows, (block + 1) * block_rows)
        query_block = query_wide[span, :]
        lane = lax.broadcasted_iota(jnp.int32, query_block.shape, 1)
        lane_head = jnp.where(
            lane < head_lanes,
            lane // CONTENT,
            (lane - head_lanes) // ROTARY - head_index * heads % (128 // ROTARY),
        )
        out_lane = lax.broadcasted_iota(jnp.int32, (block_rows, head_lanes), 1)
        result = jnp.zeros((block_rows, head_lanes), jnp.float32)
        for head in range(heads):
            chosen = jnp.where(lane_head == head, query_block, jnp.zeros_like(query_block))
            scores = lax.dot_general(
                chosen, keys[...], (((1,), (1,)), ((), ())), preferred_element_type=jnp.float32
            ) * ((CONTENT + ROTARY) ** (-0.5))
            weights = jnp.exp(scores - jnp.max(scores, -1, keepdims=True))
            total = jnp.sum(weights, -1, keepdims=True)
            summed = jnp.dot(
                weights.astype(jnp.bfloat16), values[...], preferred_element_type=jnp.float32
            )
            result = jnp.where(out_lane // VALUE == head, summed / total, result)
        attended[span, :] = result.astype(jnp.bfloat16)

    def mix():
        for start in range(0, width, stripe):
            product = jnp.dot(
                attended[...],
                output_weight_ref[:, start : start + stripe],
                preferred_element_type=jnp.float32,
            ).astype(jnp.bfloat16)
            side[:, :, own_rows:, start : start + stripe] = product.reshape(
                2, 2, own_rows, stripe
            )

    def share():
        for fetch in fetches[5:8]:
            fetch.wait()
        for route in ("core", "cross"):
            moved(tokens, 0, ep_count, route).wait_recv()
        hidden = gated_rows(
            tokens[...].reshape(group_rows, width), shared_gate_ref[...], shared_up_ref[...]
        )
        for start in range(0, width, stripe):
            product = jnp.dot(
                hidden,
                shared_down_ref[:, start : start + stripe],
                preferred_element_type=jnp.float32,
            ).astype(jnp.bfloat16)
            side[:, :, :own_rows, start : start + stripe] = product.reshape(
                2, 2, own_rows, stripe
            )

    def side_half(target_row, place):
        return remote(
            side.at[target_row, 1 - core],
            half_side.at[target_row],
            half_send.at[1, place],
            half_recv.at[1, place],
            core_peer,
        )

    near_side, outer_side = side_half(row, 0), side_half(1 - row, 1)
    side_copy = remote(
        side.at[1 - row, core], far_side, far_send.at[ep_count], far_recv.at[ep_count], y_peer
    )

    def side_exchange():
        outer_side.start()
        near_side.start()

    def side_far():
        outer_side.wait_recv()
        side[1 - row, core] = (
            side[1 - row, core].astype(jnp.float32) + half_side[1 - row].astype(jnp.float32)
        ).astype(jnp.bfloat16)

    tasks = [
        project,
        lambda: attend(0),
        lambda: attend(1),
        lambda: attend(2),
        lambda: attend(3),
        mix,
        share,
        side_exchange,
        side_far,
    ]
    for step in range(max(ep_count + 1, len(tasks))):
        if 0 < step < ep_count:
            slots_ep(step).wait_recv()
            for route in ("y", "core"):
                moved(rows, 0, step, route).start()
        if 0 < step <= ep_count:
            moved(rows, 0, step - 1, "y").wait_recv()
            moved(rows, 0, step - 1, "cross").start()
        if step < len(tasks):
            tasks[step]()
    side_copy.start()
    for fetch in fetches[8:]:
        fetch.wait()
    for route in ("core", "cross"):
        for step in range(ep_count):
            moved(rows, 0, step, route).wait_recv()

    def compute(side_core):
        for expert in range(local_experts):
            span = slice(expert * capacity, (expert + 1) * capacity)
            block = rows[:, side_core, :, span, :].reshape(2 * ep_count * capacity, width)
            hidden = gated_rows(block, gate_ref[expert], up_ref[expert])
            for start in range(0, width, stripe):
                product = jnp.dot(
                    hidden,
                    down_ref[expert, :, start : start + stripe],
                    preferred_element_type=jnp.float32,
                ).astype(jnp.bfloat16)
                part[:, side_core, :, span, start : start + stripe] = product.reshape(
                    2, ep_count, capacity, stripe
                )

    def rows_half(target_row, place):
        return remote(
            part.at[target_row, 1 - core],
            half_rows.at[target_row],
            half_send.at[0, place],
            half_recv.at[0, place],
            core_peer,
        )

    compute(1 - core)
    near, outer = rows_half(row, 0), rows_half(1 - row, 1)
    outer.start()
    near.start()
    compute(core)

    def y_copy(step):
        return remote(
            part.at[1 - row, core, step],
            far_rows.at[step],
            far_send.at[step],
            far_recv.at[step],
            y_peer,
        )

    def back_copy(step):
        return remote(
            part.at[row, core, step],
            returned.at[me],
            back_send.at[step],
            back_recv.at[step],
            (lax.rem(me + ep_count - step, ep_count), head_index),
        )

    outer.wait_recv()
    order = list(range(1, ep_count)) + [0]
    for step in order:
        part[1 - row, core, step] = (
            part[1 - row, core, step].astype(jnp.float32)
            + half_rows[1 - row, step].astype(jnp.float32)
        ).astype(jnp.bfloat16)
        y_copy(step).start()
    near.wait_recv()
    near_side.wait_recv()
    side_copy.wait_recv()
    side_total = (
        side[row, core].astype(jnp.float32)
        + half_side[row].astype(jnp.float32)
        + far_side[...].astype(jnp.float32)
    )
    both_out[0] = side_total[own_rows:].astype(jnp.bfloat16)
    for step in order:
        y_copy(step).wait_recv()
        total = (
            part[row, core, step].astype(jnp.float32)
            + half_rows[row, step].astype(jnp.float32)
            + far_rows[step].astype(jnp.float32)
        ).astype(jnp.bfloat16)
        if step > 0:
            part[row, core, step] = total
            back_copy(step).start()
        else:
            returned[me] = total
    for step in range(1, ep_count):
        back_copy(step).wait_recv()
    for start in range(0, width, stripe):
        picked = jnp.dot(
            weight_ref[...],
            returned[:, :, start : start + stripe].reshape(ep_count * slot_rows, stripe),
            preferred_element_type=jnp.float32,
        )
        picked = picked[:own_rows] + picked[own_rows : 2 * own_rows] + picked[2 * own_rows :]
        both_out[1, :, start : start + stripe] = (
            picked + side_total[:own_rows, start : start + stripe]
        ).astype(jnp.bfloat16)

    for step in range(1, ep_count):
        latent_ep(step).wait_send()
        slots_ep(step).wait_send()
        back_copy(step).wait_send()
    for route in ("y", "core", "cross"):
        moved(queries, 1, ep_count, route).wait_send()
        moved(tokens, 0, ep_count, route).wait_send()
        for step in range(ep_count):
            moved(latents, 1, step, route).wait_send()
            moved(rows, 0, step, route).wait_send()
    for copy in (near, outer, near_side, outer_side, side_copy):
        copy.wait_send()
    for step in range(ep_count):
        y_copy(step).wait_send()


def block_call(ep_count, capacity, *operands):
    query_latent, key_latent = operands[:2]
    own_rows, width = operands[5].shape
    head_lanes = operands[15].shape[0]
    slot_rows = operands[16].shape[0] * capacity
    latent_shape = (own_rows, key_latent.shape[1] + 128)
    vmem = pl.BlockSpec(memory_space=pltpu.VMEM)
    anywhere = pl.BlockSpec(memory_space=pl.ANY)

    def held(*shape):
        return pltpu.VMEM(shape, jnp.bfloat16)

    def sems(*shape):
        return pltpu.SemaphoreType.DMA(shape)

    key_rows = 4 * ep_count * own_rows
    return pl.pallas_call(
        lambda *refs: block_kernel(ep_count, capacity, *refs),
        out_shape=jax.ShapeDtypeStruct((2, own_rows, width), jnp.bfloat16),
        in_specs=[vmem] * 11 + [anywhere] * 11,
        out_specs=vmem,
        scratch_shapes=[
            held(ep_count, slot_rows, width),
            held(query_latent.shape[1], head_lanes + 128),
            held(key_latent.shape[1], 2 * head_lanes),
            held(head_lanes, width),
            held(3 * own_rows, ep_count * slot_rows),
            held(2, 2, ep_count, slot_rows, width),
            held(2, 2, ep_count, *latent_shape),
            held(2, 2, own_rows, width),
            held(2, 2, *query_latent.shape),
        ]
        + [held(*operand.shape) for operand in operands[16:]]
        + [
            held(key_rows, head_lanes + 128),
            held(key_rows, head_lanes),
            held(4 * own_rows, head_lanes + 128),
            held(4 * own_rows, head_lanes),
            held(2, 2, ep_count, slot_rows, width),
            held(2, 2, 2 * own_rows, width),
            held(2, ep_count, slot_rows, width),
            held(2, 2 * own_rows, width),
            held(ep_count, slot_rows, width),
            held(2 * own_rows, width),
            held(ep_count, slot_rows, width),
        ]
        + [sems(2, ep_count + 1)] * 8
        + [
            sems(1),
            sems(11),
            sems(2, 2),
            sems(2, 2),
            sems(ep_count + 1),
            sems(ep_count + 1),
            sems(ep_count),
            sems(ep_count),
        ],
        compiler_params=pltpu.CompilerParams(
            collective_id=0, has_side_effects=True, vmem_limit_bytes=VMEM_LIMIT
        ),
        name="block",
    )(*operands)


def shards(
    query_latent,
    key_latent,
    rotary_key,
    query_gain,
    latent_gain,
    query_content,
    query_rotary,
    key_content,
    value_weight,
    output_weight,
    expert_input,
    norm_gain,
    routes,
    route_weight,
    expert_gate,
    expert_up,
    expert_down,
    shared_gate,
    shared_up,
    shared_down,
):
    group_size = lax.axis_size("tp")
    expert_groups = lax.axis_size("ep")
    token_rows = expert_input.shape[0]
    picks = routes.shape[1]
    local_experts = expert_gate.shape[0]
    expert_total = local_experts * expert_groups
    capacity = 2 * token_rows * picks // expert_total
    if group_size != 4 or capacity % 16:
        return shards_plain(
            query_latent,
            key_latent,
            rotary_key,
            query_gain,
            latent_gain,
            query_content,
            query_rotary,
            key_content,
            value_weight,
            output_weight,
            expert_input,
            norm_gain,
            routes,
            route_weight,
            expert_gate,
            expert_up,
            expert_down,
            shared_gate,
            shared_up,
            shared_down,
        )
    group_rows_count = expert_input.shape[0] * group_size
    positions = lax.axis_index("ep") * group_rows_count + jnp.arange(
        group_rows_count, dtype=jnp.int32
    )
    frequency = rope_base ** (-jnp.arange(ROTARY // 2, dtype=jnp.float32) * 2.0 / ROTARY)
    angles = positions.astype(jnp.float32)[:, None] * jnp.tile(
        jnp.repeat(frequency, 2), 128 // ROTARY
    )[None, :]
    both = block_call(
        expert_groups,
        capacity,
        query_latent,
        key_latent,
        rotary_key.T,
        query_gain[None, :],
        latent_gain[None, :],
        expert_input,
        norm_gain[None, :],
        routes.T,
        route_weight.T,
        jnp.cos(angles),
        jnp.sin(angles),
        query_content,
        query_rotary,
        key_content,
        value_weight,
        output_weight,
        expert_gate,
        expert_up,
        expert_down,
        shared_gate,
        shared_up,
        shared_down,
    )
    return (both[0], both[1])


def solution(mesh):
    in_specs = (
        P(("ep", "tp"), None),
        P(("ep", "tp"), None),
        P(("ep", "tp"), None),
        P(),
        P(),
        P(),
        P(),
        P(),
        P(),
        P("tp", None),
        P(("ep", "tp"), None),
        P(),
        P(("ep", "tp"), None),
        P(("ep", "tp"), None),
        P("ep", None, "tp"),
        P("ep", None, "tp"),
        P("ep", "tp", None),
        P(None, "tp"),
        P(None, "tp"),
        P("tp", None),
    )
    out_specs = (P(("ep", "tp"), None), P(("ep", "tp"), None))
    return jax.shard_map(shards, mesh=mesh, in_specs=in_specs, out_specs=out_specs, check_vma=False)
```

profile of v0, /device:TPU:0, one launch (start us, length us, event | category | flops | bytes accessed | tf_op | source)
XLA Modules:
  0.0 103.8 jit_solution(753067209127568395)
XLA Ops:
  0.7 0.1 broadcast_in_dim.16
  0.7 0.1 tile.7
  0.8 0.1 mul.21
  0.9 1.2 %multiply_sine_fusion = (f32[256,128]{1,0:T(8,128)}, f32[256,128]{1,0:T(8,128)}) fusion(f32[128]{0:T(128)S(1)} %mul.21, f32[256]{0:T(256)S(1)} %add_convert_fusion), kind=kLoop, calls=%fused_computation.2 | loop fusion | flops 32768 | bytes 263680 | tf_op jit(solution)/shard_map/sin | solution.py:894
  2.2 99.7 %block.1 = bf16[2,64,2048]{2,1,0:T(8,128)(2,1)} custom-call(bf16[64,512]{1,0:T(8,128)(2,1)} %refs_0_.1, bf16[64,256]{1,0:T(8,128)(2,1)} %refs_1_.1, bf16[32,64]{1,0:T(8,128)(2,1)} %bitcast.10, f32[1,512]{1,0:T(1,128)} %bitcast.12, f32[1,256]{1,0:T(1,128)} %bitcast.13, bf16[64,2048]{1,0:T(8,128)(2,1)} %refs_5_.1, f32[1,2048]{1,0:T(1,128)} %bitcast.11, ...), custom_call_target="tpu_custom_call" | custom-call | tf_op jit(solution)/shard_map/block/pallas_call | solution.py:773
  101.9 1.9 %slice_bitcast_fusion = (bf16[64,2048]{1,0:T(8,128)(2,1)}, bf16[64,2048]{1,0:T(8,128)(2,1)}) fusion(bf16[2,64,2048]{2,1,0:T(8,128)(2,1)} %block.1), kind=kLoop, calls=%fused_computation | loop fusion | bytes 1048576 | tf_op jit(solution)/shard_map/squeeze | solution.py:907
  (3 shorter events, 0.0 us)
where the time goes:
time: 104 us
  Pallas kernels  99.7 us (96%)
  local copies, waits for them, and re-layouts  2.11 us (2%)
  other arithmetic  1.25 us (1%)
    pallas_call x1, Pallas kernels, block_call(): pl.pallas_call(lambda *refs: block_kernel(ep_count, capacity, *refs), out...  99.7 us

commit v1 on v0

v1 whole, which is shorter than its diff:
```python
import math

import jax
import jax.numpy as jnp
from jax import lax
from jax.experimental import pallas as pl
from jax.experimental.pallas import tpu as pltpu
from jax.sharding import PartitionSpec as P

HEADS = 8
CONTENT = 64
ROTARY = 32
VALUE = 64


norm_eps = 1e-06
rope_base = 10000.0


def rms_rows(entries, gain_row):
    widened = entries.astype(jnp.float32)
    return widened * lax.rsqrt(jnp.mean(widened * widened, -1, keepdims=True) + norm_eps) * gain_row


def turn_pairs(entries, positions):
    width_full = entries.shape[-1]
    frequency = rope_base ** (-jnp.arange(width_full // 2, dtype=jnp.float32) * 2.0 / width_full)
    angles = positions.astype(jnp.float32)[:, None] * frequency[None, :]
    cosine = jnp.cos(angles)[:, None, :]
    sine_part = jnp.sin(angles)[:, None, :]
    even_part = entries[..., 0::2]
    odd_part = entries[..., 1::2]
    joined = jnp.stack(
        [even_part * cosine - odd_part * sine_part, even_part * sine_part + odd_part * cosine], -1
    )
    return joined.reshape(entries.shape)


def absorb_block(carried, query_part, query_turn, key_part, key_turn, value_rows, score_scale):
    running_peak, running_total, summed = carried
    scores = jnp.einsum("qhc,khc->qhk", query_part, key_part, preferred_element_type=jnp.float32)
    scores = scores + jnp.einsum(
        "qhr,kr->qhk", query_turn, key_turn, preferred_element_type=jnp.float32
    )
    scores = scores * score_scale
    new_peak = jnp.maximum(running_peak, jnp.max(scores, -1))
    factor = jnp.exp(running_peak - new_peak)
    weights = jnp.exp(scores - new_peak[..., None])
    running_total = running_total * factor + jnp.sum(weights, -1)
    summed = summed * factor[..., None] + jnp.einsum(
        "qhk,khv->qhv", weights.astype(jnp.bfloat16), value_rows, preferred_element_type=jnp.float32
    )
    return (new_peak, running_total, summed)


def absorb_piece(carried, query_part, query_turn, key_part, key_turn, value_rows, score_scale):
    row_count = key_part.shape[0]
    key_block = math.gcd(row_count, 2048)
    if key_block == row_count:
        return absorb_block(
            carried, query_part, query_turn, key_part, key_turn, value_rows, score_scale
        )
    block_count = row_count // key_block

    def advance(state, pieces):
        return (
            absorb_block(
                state, query_part, query_turn, pieces[0], pieces[1], pieces[2], score_scale
            ),
            None,
        )

    stacked = (
        key_part.reshape((block_count, key_block) + key_part.shape[1:]),
        key_turn.reshape(block_count, key_block, key_turn.shape[1]),
        value_rows.reshape((block_count, key_block) + value_rows.shape[1:]),
    )
    carried, ignored = lax.scan(advance, carried, stacked)
    return carried


def expand_keys(latent_rows, key_columns, value_columns, head_local):
    row_count = latent_rows.shape[0]
    key_part = (
        jnp.dot(latent_rows, key_columns, preferred_element_type=jnp.float32)
        .astype(jnp.bfloat16)
        .reshape(row_count, head_local, CONTENT)
    )
    value_rows = (
        jnp.dot(latent_rows, value_columns, preferred_element_type=jnp.float32)
        .astype(jnp.bfloat16)
        .reshape(row_count, head_local, VALUE)
    )
    return (key_part, value_rows)


def expert_terms(row_block, gate_weight, up_weight, down_weight):
    gated = jnp.einsum("secd,edf->secf", row_block, gate_weight, preferred_element_type=jnp.float32)
    lifted = jnp.einsum("secd,edf->secf", row_block, up_weight, preferred_element_type=jnp.float32)
    hidden = (jax.nn.silu(gated) * lifted).astype(jnp.bfloat16)
    return jnp.einsum("secf,efd->secd", hidden, down_weight, preferred_element_type=jnp.float32)


def shared_terms(row_block, gate_weight, up_weight, down_weight):
    gated = jnp.dot(row_block, gate_weight, preferred_element_type=jnp.float32)
    lifted = jnp.dot(row_block, up_weight, preferred_element_type=jnp.float32)
    hidden = (jax.nn.silu(gated) * lifted).astype(jnp.bfloat16)
    return jnp.dot(hidden, down_weight, preferred_element_type=jnp.float32)


def shards_plain(
    query_latent,
    key_latent,
    rotary_key,
    query_gain,
    latent_gain,
    query_content,
    query_rotary,
    key_content,
    value_weight,
    output_weight,
    expert_input,
    norm_gain,
    routes,
    route_weight,
    expert_gate,
    expert_up,
    expert_down,
    shared_gate,
    shared_up,
    shared_down,
):
    group_size = lax.axis_size("tp")
    expert_groups = lax.axis_size("ep")
    own_rows = query_latent.shape[0]
    head_local = HEADS // group_size
    head_index = lax.axis_index("tp")
    group_rows_count = own_rows * group_size
    group_start = lax.axis_index("ep") * group_rows_count
    own_start = group_start + head_index * own_rows
    score_scale = (CONTENT + ROTARY) ** (-0.5)
    query_normed = rms_rows(query_latent, query_gain).astype(jnp.bfloat16)
    latent_normed = rms_rows(key_latent, latent_gain).astype(jnp.bfloat16)
    own_positions = own_start + jnp.arange(own_rows, dtype=jnp.int32)
    key_turned = turn_pairs(rotary_key.astype(jnp.float32)[:, None, :], own_positions)[
        :, 0, :
    ].astype(jnp.bfloat16)
    token_rows = expert_input.shape[0]
    picks = routes.shape[1]
    local_experts = expert_gate.shape[0]
    expert_total = local_experts * expert_groups
    capacity = 2 * token_rows * picks // expert_total
    slot_total = expert_total * capacity
    model_width = expert_input.shape[1]
    expert_normed = rms_rows(expert_input, norm_gain).astype(jnp.bfloat16)
    flat_routes = routes.reshape(-1)
    marks = (flat_routes[:, None] == jnp.arange(expert_total, dtype=jnp.int32)[None, :]).astype(
        jnp.int32
    )
    ranks = jnp.sum((jnp.cumsum(marks, 0) - marks) * marks, 1)
    targets = flat_routes * capacity + ranks
    picker = (jnp.arange(slot_total, dtype=jnp.int32)[:, None] == targets[None, :]).astype(
        jnp.int32
    )
    picker = jnp.sum(picker.reshape(slot_total, token_rows, picks), 2).astype(jnp.bfloat16)
    outgoing = jnp.dot(picker, expert_normed, preferred_element_type=jnp.float32).astype(
        jnp.bfloat16
    )
    outgoing = outgoing.reshape(expert_groups, local_experts, capacity, model_width)
    received = lax.all_to_all(outgoing, "ep", split_axis=0, concat_axis=0, tiled=True)
    group_query, group_latent, group_turn, gathered_rows, gathered_tokens = (
        lax.all_gather(query_normed, "tp", axis=0, tiled=True),
        lax.all_gather(latent_normed, "tp", axis=0, tiled=True),
        lax.all_gather(key_turned, "tp", axis=0, tiled=True),
        lax.all_gather(received, "tp", axis=0, tiled=True),
        lax.all_gather(expert_normed, "tp", axis=0, tiled=True),
    )
    positions = group_start + jnp.arange(group_rows_count, dtype=jnp.int32)
    content_columns = lax.dynamic_slice_in_dim(
        query_content, head_index * head_local * CONTENT, head_local * CONTENT, 1
    )
    rotary_columns = lax.dynamic_slice_in_dim(
        query_rotary, head_index * head_local * ROTARY, head_local * ROTARY, 1
    )
    query_part = (
        jnp.dot(group_query, content_columns, preferred_element_type=jnp.float32)
        .astype(jnp.bfloat16)
        .reshape(group_rows_count, head_local, CONTENT)
    )
    query_turn = turn_pairs(
        jnp.dot(group_query, rotary_columns, preferred_element_type=jnp.float32).reshape(
            group_rows_count, head_local, ROTARY
        ),
        positions,
    ).astype(jnp.bfloat16)
    key_columns = lax.dynamic_slice_in_dim(
        key_content, head_index * head_local * CONTENT, head_local * CONTENT, 1
    )
    value_columns = lax.dynamic_slice_in_dim(
        value_weight, head_index * head_local * VALUE, head_local * VALUE, 1
    )
    carry_start = (
        jnp.full((group_rows_count, head_local), -jnp.inf, jnp.float32),
        jnp.zeros((group_rows_count, head_local), jnp.float32),
        jnp.zeros((group_rows_count, head_local, VALUE), jnp.float32),
    )
    key_part, value_rows = expand_keys(
        lax.all_gather(group_latent, "ep", axis=0, tiled=True),
        key_columns,
        value_columns,
        head_local,
    )
    running_peak, running_total, summed = absorb_piece(
        carry_start,
        query_part,
        query_turn,
        key_part,
        lax.all_gather(group_turn, "ep", axis=0, tiled=True),
        value_rows,
        score_scale,
    )
    attended = (
        (summed / running_total[..., None])
        .astype(jnp.bfloat16)
        .reshape(group_rows_count, head_local * VALUE)
    )
    routed_term = expert_terms(gathered_rows, expert_gate, expert_up, expert_down)
    shared_term = shared_terms(gathered_tokens, shared_gate, shared_up, shared_down)
    mixer_term = jnp.dot(attended, output_weight, preferred_element_type=jnp.float32)
    mixer_sum, routed_sum, shared_sum = (
        lax.psum_scatter(
            mixer_term.astype(jnp.bfloat16), "tp", scatter_dimension=0, tiled=True
        ).astype(jnp.float32),
        lax.psum_scatter(
            routed_term.astype(jnp.bfloat16), "tp", scatter_dimension=0, tiled=True
        ).astype(jnp.float32),
        lax.psum_scatter(
            shared_term.astype(jnp.bfloat16), "tp", scatter_dimension=0, tiled=True
        ).astype(jnp.float32),
    )
    mixer_out = mixer_sum.astype(jnp.bfloat16)
    returned = lax.all_to_all(
        routed_sum.astype(jnp.bfloat16), "ep", split_axis=0, concat_axis=0, tiled=True
    )
    returned = returned.reshape(slot_total, model_width)
    picked = jnp.take(returned, targets, axis=0).reshape(token_rows, picks, model_width)
    combined = jnp.sum(route_weight[..., None] * picked.astype(jnp.float32), 1) + shared_sum
    expert_out = combined.astype(jnp.bfloat16)
    return (mixer_out, expert_out)


MESH = pl.DeviceIdType.MESH
VMEM_LIMIT = 60 * 1024 * 1024
NEAR = 4


def fits_kernel(ep_count, slot_rows):
    power = ep_count & (ep_count - 1) == 0
    return power and ep_count > NEAR and NEAR * slot_rows % 128 == 0


def flip(place, bits):
    flipped = place
    bit = 1
    while bit <= bits:
        if bits & bit:
            flipped = flipped + bit * (1 - 2 * (place // bit % 2))
        bit *= 2
    return flipped


def greet(ep_count, me, head_index):
    barrier = pltpu.get_barrier_semaphore()
    for step in range(1, ep_count):
        pl.semaphore_signal(
            barrier, inc=1, device_id=(flip(me, step), head_index), device_id_type=MESH
        )
    row, core = head_index // 2, head_index % 2
    for other in ((1 - row) * 2 + core, row * 2 + 1 - core):
        pl.semaphore_signal(barrier, inc=1, device_id=(me, other), device_id_type=MESH)
    pl.semaphore_wait(barrier, ep_count + 1)


def gated_rows(rows, gate_weight, up_weight):
    gated = jnp.dot(rows, gate_weight, preferred_element_type=jnp.float32)
    lifted = jnp.dot(rows, up_weight, preferred_element_type=jnp.float32)
    return (gated / (1.0 + jnp.exp(-gated)) * lifted).astype(jnp.bfloat16)


def wide(entries):
    return entries.astype(jnp.float32)


def narrow(entries):
    return entries.astype(jnp.bfloat16)


def choose_slots(routes, weights, expert_total, capacity, first_slot, slot_count):
    own_rows = routes.shape[0]
    expert_lane = lax.broadcasted_iota(jnp.int32, (own_rows, expert_total), 1)
    named = [
        jnp.where(routes[:, pick : pick + 1] == expert_lane, 1.0, 0.0)
        for pick in range(routes.shape[1])
    ]
    earlier = narrow(
        jnp.where(
            lax.broadcasted_iota(jnp.int32, (own_rows, own_rows), 0)
            > lax.broadcasted_iota(jnp.int32, (own_rows, own_rows), 1),
            1.0,
            0.0,
        )
    )
    ahead = jnp.dot(earlier, narrow(sum(named)), preferred_element_type=jnp.float32)
    slot_lane = lax.broadcasted_iota(jnp.int32, (own_rows, slot_count), 1) + first_slot
    picker = jnp.zeros(slot_lane.shape, jnp.float32)
    weight = jnp.zeros(slot_lane.shape, jnp.float32)
    for pick, marks in enumerate(named):
        rank = jnp.sum(ahead * marks, 1, keepdims=True).astype(jnp.int32)
        chosen = slot_lane == routes[:, pick : pick + 1] * capacity + rank
        picker = jnp.where(chosen, 1.0, picker)
        weight = jnp.where(chosen, weights[:, pick : pick + 1], weight)
    return narrow(picker.T), weight


def store_split(target, weight):
    own_rows = weight.shape[0]
    high = narrow(weight)
    rest = weight - wide(high)
    middle = narrow(rest)
    target[:own_rows] = high
    target[own_rows : 2 * own_rows] = middle
    target[2 * own_rows :] = narrow(rest - wide(middle))


def weighted_rows(split_weight, entries):
    picked = jnp.dot(split_weight, entries, preferred_element_type=jnp.float32)
    own_rows = picked.shape[0] // 3
    return picked[:own_rows] + picked[own_rows : 2 * own_rows] + picked[2 * own_rows :]


def block_kernel(
    ep_count,
    capacity,
    query_latent_ref,
    key_latent_ref,
    rotary_key_ref,
    query_gain_ref,
    latent_gain_ref,
    expert_input_ref,
    norm_gain_ref,
    routes_ref,
    route_weight_ref,
    cosine_ref,
    sine_ref,
    query_content_hbm,
    query_rotary_hbm,
    key_content_hbm,
    value_weight_hbm,
    output_weight_hbm,
    gate_hbm,
    up_hbm,
    down_hbm,
    shared_gate_hbm,
    shared_up_hbm,
    shared_down_hbm,
    both_out,
    slots_ref,
    peer_slots_ref,
    query_columns_ref,
    latent_columns_ref,
    output_weight_ref,
    weight_ref,
    peer_weight_ref,
    rows,
    latents,
    tokens,
    queries,
    gate_ref,
    up_ref,
    down_ref,
    shared_gate_ref,
    shared_up_ref,
    shared_down_ref,
    keys,
    values,
    query_wide,
    attended,
    part,
    half_rows,
    far_rows,
    returned,
    returned_peer,
    mixed,
    half_mixed,
    far_mixed,
    shared,
    half_shared,
    far_shared,
    info_ref,
    peer_info_ref,
    own_sum,
    own_stats,
    sent_sum,
    far_sum,
    ep_send,
    ep_recv,
    y_send,
    y_recv,
    core_send,
    core_recv,
    cross_send,
    cross_recv,
    peer_send,
    peer_recv,
    back_send,
    back_recv,
    far_send,
    far_recv,
    half_send,
    half_recv,
    side_send,
    side_recv,
    own_sem,
    weight_sem,
):
    me = lax.axis_index("ep")
    head_index = lax.axis_index("tp")
    row, core = head_index // 2, head_index % 2
    y_peer = (me, (1 - row) * 2 + core)
    core_peer = (me, row * 2 + 1 - core)
    local_experts = gate_ref.shape[0]
    width = rows.shape[-1]
    own_rows = tokens.shape[2]
    slot_rows = rows.shape[3]
    group_rows = attended.shape[0]
    picks = routes_ref.shape[0]
    stripe = math.gcd(width, 512)
    far_steps = range(NEAR, ep_count)
    near_place = me % NEAR

    def peer(step):
        return (flip(me, step), head_index)

    def remote(source, target, send_sem, recv_sem, device):
        return pltpu.make_async_remote_copy(
            src_ref=source,
            dst_ref=target,
            send_sem=send_sem,
            recv_sem=recv_sem,
            device_id=device,
            device_id_type=MESH,
        )

    head_lanes = attended.shape[1]
    heads = head_lanes // VALUE
    fetch_list = []
    for side in range(2):
        side_index = (row if side == 0 else 1 - row) * 2 + core
        columns = pl.ds(pl.multiple_of(side_index * head_lanes, head_lanes), head_lanes)
        turn_columns = pl.ds(pl.multiple_of(side_index * heads * ROTARY // 128 * 128, 128), 128)
        fetch_list += [
            (query_content_hbm.at[:, columns], query_columns_ref.at[side, :, :head_lanes]),
            (query_rotary_hbm.at[:, turn_columns], query_columns_ref.at[side, :, head_lanes:]),
            (key_content_hbm.at[:, columns], latent_columns_ref.at[side, :, :head_lanes]),
            (value_weight_hbm.at[:, columns], latent_columns_ref.at[side, :, head_lanes:]),
        ]
    fetch_list += [
        (output_weight_hbm, output_weight_ref),
        (shared_gate_hbm, shared_gate_ref),
        (shared_up_hbm, shared_up_ref),
        (shared_down_hbm, shared_down_ref),
        (gate_hbm, gate_ref),
        (up_hbm, up_ref),
        (down_hbm, down_ref),
    ]
    fetches = [
        pltpu.make_async_copy(source, target, weight_sem.at[place])
        for place, (source, target) in enumerate(fetch_list)
    ]
    for fetch in fetches:
        fetch.start()

    def turn(entries, cosine, sine):
        lane = lax.broadcasted_iota(jnp.int32, entries.shape, 1)
        crossed = jnp.where(
            lane % 2 == 0, -pltpu.roll(entries, 127, 1), pltpu.roll(entries, 1, 1)
        )
        return narrow(entries * cosine + crossed * sine)

    rank_width = key_latent_ref.shape[1]
    latents[core, 0, :, :rank_width] = narrow(rms_rows(key_latent_ref[...], latent_gain_ref[...]))
    repeats = narrow(
        jnp.where(
            lax.broadcasted_iota(jnp.int32, (ROTARY, 128), 0)
            == lax.broadcasted_iota(jnp.int32, (ROTARY, 128), 1) % ROTARY,
            1.0,
            0.0,
        )
    )
    own_span = pl.ds(pl.multiple_of(head_index * own_rows, own_rows), own_rows)
    latents[core, 0, :, rank_width:] = turn(
        lax.dot_general(
            rotary_key_ref[...],
            repeats,
            (((0,), (0,)), ((), ())),
            preferred_element_type=jnp.float32,
        ),
        cosine_ref[own_span, :],
        sine_ref[own_span, :],
    )
    queries[row, core] = narrow(rms_rows(query_latent_ref[...], query_gain_ref[...]))
    info_ref[...] = jnp.zeros(info_ref.shape, jnp.float32)
    info_ref[:picks, :own_rows] = routes_ref[...].astype(jnp.float32)
    info_ref[picks : 2 * picks, :own_rows] = route_weight_ref[...]
    greet(ep_count, me, head_index)

    def latent_ep(step):
        if step % 2 == 0:
            return remote(
                latents.at[core, 0],
                latents.at[core, step],
                ep_send.at[1, step],
                ep_recv.at[1, step],
                peer(step),
            )
        return remote(
            latents.at[core, step - 1],
            latents.at[core, step],
            ep_send.at[1, step],
            ep_recv.at[1, step],
            peer(1),
        )

    def latent_core(step):
        return remote(
            latents.at[core, step],
            latents.at[core, step],
            core_send.at[1, step],
            core_recv.at[1, step],
            core_peer,
        )

    def slots_ep(step):
        return remote(
            slots_ref.at[flip(me, step)],
            rows.at[row, core, step],
            ep_send.at[0, step],
            ep_recv.at[0, step],
            peer(step),
        )

    def peer_slots_ep(step):
        return remote(
            peer_slots_ref.at[flip(near_place, step)],
            rows.at[1 - row, core, step],
            peer_send.at[0, step],
            peer_recv.at[0, step],
            peer(step),
        )

    routes_of = {
        "y": (row, y_send, y_recv, y_peer),
        "core": (row, core_send, core_recv, core_peer),
        "cross": (1 - row, cross_send, cross_recv, core_peer),
    }

    def moved_rows(step, route):
        origin_row, send_sem, recv_sem, device = routes_of[route]
        block = rows.at[origin_row, core, step]
        return remote(block, block, send_sem.at[0, step], recv_sem.at[0, step], device)

    def moved(buffer, place, route):
        origin_row, send_sem, recv_sem, device = routes_of[route]
        block = buffer.at[origin_row, core]
        return remote(
            block, block, send_sem.at[place, ep_count], recv_sem.at[place, ep_count], device
        )

    info_y = remote(
        info_ref, peer_info_ref, y_send.at[0, 0], y_recv.at[0, 0], y_peer
    )
    for step in range(1, ep_count):
        if step == 1 or step % 2 == 0:
            latent_ep(step).start()
    latent_core(0).start()
    info_y.start()
    for route in ("y", "core"):
        moved(queries, 1, route).start()
    expert_normed = narrow(rms_rows(expert_input_ref[...], norm_gain_ref[...]))
    tokens[row, core] = expert_normed
    for route in ("y", "core"):
        moved(tokens, 0, route).start()
    expert_total = local_experts * ep_count
    picker, weight = choose_slots(
        routes_ref[...].T, route_weight_ref[...].T, expert_total, capacity, 0, ep_count * slot_rows
    )
    store_split(weight_ref, weight)

    def fill(target, chooser, origin_row):
        for start in range(0, width, stripe):
            target[:, :, start : start + stripe] = narrow(
                jnp.dot(
                    chooser,
                    tokens[origin_row, core, :, start : start + stripe],
                    preferred_element_type=jnp.float32,
                )
            ).reshape(target.shape[0], slot_rows, stripe)

    fill(slots_ref, picker, row)
    for step in range(1, ep_count):
        slots_ep(step).start()
    own_slots = pltpu.make_async_copy(slots_ref.at[me], rows.at[row, core, 0], own_sem.at[0])
    own_slots.start()
    own_slots.wait()
    moved_rows(0, "core").start()

    def pass_latents(steps):
        for step in steps:
            latent_ep(step).wait_recv()
            if step % 2 == 0:
                latent_ep(step + 1).start()
            latent_core(step).start()

    pass_latents(range(2, ep_count, 2))
    moved(queries, 1, "y").wait_recv()
    moved(queries, 1, "cross").start()
    info_y.wait_recv()
    peer_picker, peer_weight = choose_slots(
        peer_info_ref[:picks, :own_rows].T.astype(jnp.int32),
        peer_info_ref[picks : 2 * picks, :own_rows].T,
        expert_total,
        capacity,
        me // NEAR * NEAR * slot_rows,
        NEAR * slot_rows,
    )
    store_split(peer_weight_ref, peer_weight)
    moved(tokens, 0, "y").wait_recv()
    moved(tokens, 0, "cross").start()
    fill(peer_slots_ref, peer_picker, 1 - row)
    for step in range(1, NEAR):
        peer_slots_ep(step).start()
    peer_own = pltpu.make_async_copy(
        peer_slots_ref.at[near_place], rows.at[1 - row, core, 0], own_sem.at[1]
    )
    peer_own.start()
    peer_own.wait()
    moved_rows(0, "cross").start()
    pass_latents(range(1, ep_count, 2))
    for route in ("core", "cross"):
        moved(queries, 1, route).wait_recv()
    for step in range(ep_count):
        latent_core(step).wait_recv()

    def project():
        for fetch in fetches[:8]:
            fetch.wait()
        query_rows = queries[...].reshape(group_rows, queries.shape[-1])
        for side in range(2):
            projected = jnp.dot(
                query_rows, query_columns_ref[side], preferred_element_type=jnp.float32
            )
            query_wide[side, :, :head_lanes] = narrow(projected[:, :head_lanes])
            query_wide[side, :, head_lanes:] = turn(
                projected[:, head_lanes:], cosine_ref[...], sine_ref[...]
            )
        for block in range(2):
            packed = latents[block].reshape(ep_count * own_rows, latents.shape[-1])
            span = slice(block * ep_count * own_rows, (block + 1) * ep_count * own_rows)
            for side in range(2):
                expanded = narrow(
                    jnp.dot(
                        packed[:, :rank_width],
                        latent_columns_ref[side],
                        preferred_element_type=jnp.float32,
                    )
                )
                keys[side, span, :head_lanes] = expanded[:, :head_lanes]
                keys[side, span, head_lanes:] = packed[:, rank_width:]
                values[side, span, :] = expanded[:, head_lanes:]

    block_rows = group_rows // 2

    def attend(side, block):
        span = slice(block * block_rows, (block + 1) * block_rows)
        query_block = query_wide[side, span, :]
        lane = lax.broadcasted_iota(jnp.int32, query_block.shape, 1)
        lane_head = jnp.where(
            lane < head_lanes,
            lane // CONTENT,
            (lane - head_lanes) // ROTARY - core * heads % (128 // ROTARY),
        )
        out_lane = lax.broadcasted_iota(jnp.int32, (block_rows, head_lanes), 1)
        result = jnp.zeros((block_rows, head_lanes), jnp.float32)
        stats = jnp.zeros((block_rows, head_lanes), jnp.float32)
        for head in range(heads):
            chosen = jnp.where(lane_head == head, query_block, jnp.zeros_like(query_block))
            scores = lax.dot_general(
                chosen, keys[side], (((1,), (1,)), ((), ())), preferred_element_type=jnp.float32
            ) * ((CONTENT + ROTARY) ** (-0.5))
            peak = jnp.max(scores, -1, keepdims=True)
            weights = jnp.exp(scores - peak)
            total = jnp.sum(weights, -1, keepdims=True)
            summed = jnp.dot(narrow(weights), values[side], preferred_element_type=jnp.float32)
            result = jnp.where(out_lane // VALUE == head, summed, result)
            stats = jnp.where(out_lane == 2 * head, peak, stats)
            stats = jnp.where(out_lane == 2 * head + 1, total, stats)
        if side == 0:
            own_sum[span, :] = result
            own_stats[span, :] = stats
        else:
            sent_sum[span, :] = result
            sent_sum[group_rows + 8 * block : group_rows + 8 * block + 8, :] = stats.T[:8]

    sum_y = remote(sent_sum, far_sum, y_send.at[1, 0], y_recv.at[1, 0], y_peer)

    def merge():
        sum_y.wait_recv()
        out_lane = lax.broadcasted_iota(jnp.int32, (block_rows, head_lanes), 1)
        for block in range(2):
            span = slice(block * block_rows, (block + 1) * block_rows)
            here = own_stats[span, :]
            there = far_sum[group_rows + 8 * block : group_rows + 8 * block + 8, :].T
            result = jnp.zeros((block_rows, head_lanes), jnp.float32)
            for head in range(heads):
                peak_here, total_here = here[:, 2 * head : 2 * head + 1], here[:, 2 * head + 1 : 2 * head + 2]
                peak_there, total_there = there[:, 2 * head : 2 * head + 1], there[:, 2 * head + 1 : 2 * head + 2]
                peak = jnp.maximum(peak_here, peak_there)
                factor_here = jnp.exp(peak_here - peak)
                factor_there = jnp.exp(peak_there - peak)
                total = total_here * factor_here + total_there * factor_there
                summed = own_sum[span, :] * factor_here + far_sum[span, :] * factor_there
                result = jnp.where(out_lane // VALUE == head, summed / total, result)
            attended[span, :] = narrow(result)

    def mix():
        fetches[8].wait()
        for start in range(0, width, stripe):
            product = narrow(
                jnp.dot(
                    attended[...],
                    output_weight_ref[:, start : start + stripe],
                    preferred_element_type=jnp.float32,
                )
            )
            mixed[:, :, :, start : start + stripe] = product.reshape(2, 2, own_rows, stripe)

    def share():
        for fetch in fetches[9:12]:
            fetch.wait()
        for route in ("core", "cross"):
            moved(tokens, 0, route).wait_recv()
        hidden = gated_rows(
            tokens[...].reshape(group_rows, width), shared_gate_ref[...], shared_up_ref[...]
        )
        for start in range(0, width, stripe):
            product = narrow(
                jnp.dot(
                    hidden,
                    shared_down_ref[:, start : start + stripe],
                    preferred_element_type=jnp.float32,
                )
            )
            shared[:, :, :, start : start + stripe] = product.reshape(2, 2, own_rows, stripe)

    shared_half = remote(
        shared.at[:, 1 - core], half_shared, side_send.at[0], side_recv.at[0], core_peer
    )
    mixed_half = remote(
        mixed.at[:, 1 - core], half_mixed, side_send.at[1], side_recv.at[1], core_peer
    )
    shared_y = remote(
        shared.at[1 - row, core], far_shared, side_send.at[2], side_recv.at[2], y_peer
    )
    mixed_y = remote(mixed.at[1 - row, core], far_mixed, side_send.at[3], side_recv.at[3], y_peer)

    def mixed_far():
        mixed_half.wait_recv()
        mixed[1 - row, core] = narrow(wide(mixed[1 - row, core]) + wide(half_mixed[1 - row]))
        mixed_y.start()

    def arrive(step):
        slots_ep(step).wait_recv()
        if step >= NEAR:
            moved_rows(step, "y").start()
        moved_rows(step, "core").start()

    def arrive_peer(step):
        if step >= NEAR:
            moved_rows(step, "y").wait_recv()
        else:
            peer_slots_ep(step).wait_recv()
        moved_rows(step, "cross").start()

    project()
    arrive(1)
    attend(1, 0)
    arrive(2)
    arrive(3)
    attend(1, 1)
    sum_y.start()
    arrive(4)
    attend(0, 0)
    arrive(5)
    arrive_peer(1)
    arrive_peer(4)
    attend(0, 1)
    arrive(6)
    arrive_peer(5)
    merge()
    mix()
    mixed_half.start()
    for step in range(7, ep_count):
        arrive(step)
    arrive_peer(2)
    arrive_peer(3)
    share()
    shared_half.start()
    for step in range(6, ep_count):
        arrive_peer(step)
    mixed_far()

    for fetch in fetches[12:]:
        fetch.wait()

    def spans(expert):
        return slice(expert * capacity, (expert + 1) * capacity)

    def compute(first, last, expert):
        span = spans(expert)
        block = rows[:, :, first:last, span, :].reshape(4 * (last - first) * capacity, width)
        hidden = gated_rows(block, gate_ref[expert], up_ref[expert])
        for start in range(0, width, stripe):
            product = narrow(
                jnp.dot(
                    hidden,
                    down_ref[expert, :, start : start + stripe],
                    preferred_element_type=jnp.float32,
                )
            )
            part[:, :, first:last, span, start : start + stripe] = product.reshape(
                2, 2, last - first, capacity, stripe
            )

    def near_half():
        return remote(
            part.at[:, 1 - core, :NEAR],
            half_rows.at[:, :NEAR],
            half_send.at[local_experts],
            half_recv.at[local_experts],
            core_peer,
        )

    def far_half(expert):
        return remote(
            part.at[:, 1 - core, NEAR:, spans(expert)],
            half_rows.at[:, NEAR:, spans(expert)],
            half_send.at[expert],
            half_recv.at[expert],
            core_peer,
        )

    def back_near(step):
        return remote(
            part.at[row, core, step],
            returned.at[me],
            back_send.at[0, step],
            back_recv.at[0, step],
            peer(step),
        )

    def back_peer(step):
        return remote(
            part.at[1 - row, core, step],
            returned_peer.at[near_place],
            peer_send.at[1, step],
            peer_recv.at[1, step],
            peer(step),
        )

    def back_far(step, expert):
        return remote(
            part.at[row, core, step, spans(expert)],
            returned.at[me, spans(expert)],
            back_send.at[expert, step],
            back_recv.at[expert, step],
            peer(step),
        )

    def y_copy(step, expert):
        return remote(
            part.at[1 - row, core, step, spans(expert)],
            far_rows.at[step - NEAR, spans(expert)],
            far_send.at[expert, step],
            far_recv.at[expert, step],
            y_peer,
        )

    def settle_near():
        near_half().wait_recv()
        for step in list(range(1, NEAR)) + [0]:
            outer = narrow(wide(part[1 - row, core, step]) + wide(half_rows[1 - row, step]))
            if step:
                part[1 - row, core, step] = outer
                back_peer(step).start()
            else:
                returned_peer[near_place] = outer
            total = narrow(wide(part[row, core, step]) + wide(half_rows[row, step]))
            if step:
                part[row, core, step] = total
                back_near(step).start()
            else:
                returned[me] = total

    def settle_outer(expert):
        far_half(expert).wait_recv()
        span = spans(expert)
        for step in far_steps:
            part[1 - row, core, step, span] = narrow(
                wide(part[1 - row, core, step, span]) + wide(half_rows[1 - row, step, span])
            )
            y_copy(step, expert).start()

    def settle_far(expert):
        span = spans(expert)
        for step in far_steps:
            y_copy(step, expert).wait_recv()
            part[row, core, step, span] = narrow(
                wide(part[row, core, step, span])
                + wide(half_rows[row, step, span])
                + wide(far_rows[step - NEAR, span])
            )
            back_far(step, expert).start()

    def wait_rows(steps):
        for step in steps:
            for route in ("core", "cross"):
                moved_rows(step, route).wait_recv()

    wait_rows(range(NEAR))
    for expert in range(local_experts):
        compute(0, NEAR, expert)
    near_half().start()
    wait_rows(far_steps)
    for expert in range(local_experts):
        compute(NEAR, ep_count, expert)
        far_half(expert).start()
        if expert == 0:
            settle_near()
        else:
            settle_outer(expert - 1)
    settle_outer(local_experts - 1)
    for step in range(1, NEAR):
        back_peer(step).wait_recv()
    shared_half.wait_recv()
    for start in range(0, width, stripe):
        cut = slice(start, start + stripe)
        shared[1 - row, core, :, cut] = narrow(
            weighted_rows(
                peer_weight_ref[...],
                returned_peer[:, :, cut].reshape(NEAR * slot_rows, stripe),
            )
            + wide(shared[1 - row, core, :, cut])
            + wide(half_shared[1 - row, :, cut])
        )
    shared_y.start()
    for expert in range(local_experts):
        settle_far(expert)
    mixed_y.wait_recv()
    both_out[0] = narrow(wide(mixed[row, core]) + wide(half_mixed[row]) + wide(far_mixed[...]))
    shared_y.wait_recv()
    for step in range(1, NEAR):
        back_near(step).wait_recv()
    for expert in range(local_experts):
        for step in far_steps:
            back_far(step, expert).wait_recv()
    for start in range(0, width, stripe):
        cut = slice(start, start + stripe)
        both_out[1, :, cut] = narrow(
            weighted_rows(
                weight_ref[...], returned[:, :, cut].reshape(ep_count * slot_rows, stripe)
            )
            + wide(shared[row, core, :, cut])
            + wide(half_shared[row, :, cut])
            + wide(far_shared[:, cut])
        )

    for step in range(1, ep_count):
        latent_ep(step).wait_send()
        slots_ep(step).wait_send()
    for step in range(ep_count):
        latent_core(step).wait_send()
        for route in ("core", "cross"):
            moved_rows(step, route).wait_send()
    for step in range(1, NEAR):
        peer_slots_ep(step).wait_send()
        back_near(step).wait_send()
        back_peer(step).wait_send()
    for step in far_steps:
        moved_rows(step, "y").wait_send()
        for expert in range(local_experts):
            back_far(step, expert).wait_send()
            y_copy(step, expert).wait_send()
    for route in ("y", "core", "cross"):
        moved(queries, 1, route).wait_send()
        moved(tokens, 0, route).wait_send()
    for expert in range(local_experts):
        far_half(expert).wait_send()
    for copy in (info_y, sum_y, near_half(), shared_half, mixed_half, shared_y, mixed_y):
        copy.wait_send()


def block_call(ep_count, capacity, *operands):
    query_latent, key_latent = operands[:2]
    own_rows, width = operands[5].shape
    head_lanes = operands[15].shape[0]
    local_experts = operands[16].shape[0]
    slot_rows = local_experts * capacity
    latent_shape = (own_rows, key_latent.shape[1] + 128)
    vmem = pl.BlockSpec(memory_space=pltpu.VMEM)
    anywhere = pl.BlockSpec(memory_space=pl.ANY)

    def held(*shape):
        return pltpu.VMEM(shape, jnp.bfloat16)

    def precise(*shape):
        return pltpu.VMEM(shape, jnp.float32)

    def sems(*shape):
        return pltpu.SemaphoreType.DMA(shape)

    group_rows = 4 * own_rows
    key_rows = 2 * ep_count * own_rows
    row_block = (slot_rows, width)
    side = (own_rows, width)
    return pl.pallas_call(
        lambda *refs: block_kernel(ep_count, capacity, *refs),
        out_shape=jax.ShapeDtypeStruct((2, own_rows, width), jnp.bfloat16),
        in_specs=[vmem] * 11 + [anywhere] * 11,
        out_specs=vmem,
        scratch_shapes=[
            held(ep_count, *row_block),
            held(NEAR, *row_block),
            held(2, query_latent.shape[1], head_lanes + 128),
            held(2, key_latent.shape[1], 2 * head_lanes),
            held(head_lanes, width),
            held(3 * own_rows, ep_count * slot_rows),
            held(3 * own_rows, NEAR * slot_rows),
            held(2, 2, ep_count, *row_block),
            held(2, ep_count, *latent_shape),
            held(2, 2, *side),
            held(2, 2, *query_latent.shape),
        ]
        + [held(*operand.shape) for operand in operands[16:]]
        + [
            held(2, key_rows, head_lanes + 128),
            held(2, key_rows, head_lanes),
            held(2, group_rows, head_lanes + 128),
            held(group_rows, head_lanes),
            held(2, 2, ep_count, *row_block),
            held(2, ep_count, *row_block),
            held(ep_count - NEAR, *row_block),
            held(ep_count, *row_block),
            held(NEAR, *row_block),
            held(2, 2, *side),
            held(2, *side),
            held(*side),
            held(2, 2, *side),
            held(2, *side),
            held(*side),
            precise(8, 128),
            precise(8, 128),
            precise(group_rows, head_lanes),
            precise(group_rows, head_lanes),
            precise(group_rows + 16, head_lanes),
            precise(group_rows + 16, head_lanes),
        ]
        + [sems(2, ep_count + 1)] * 8
        + [sems(2, NEAR)] * 2
        + [sems(local_experts, ep_count)] * 4
        + [sems(local_experts + 1)] * 2
        + [sems(4)] * 2
        + [sems(2), sems(15)],
        compiler_params=pltpu.CompilerParams(
            collective_id=0, has_side_effects=True, vmem_limit_bytes=VMEM_LIMIT
        ),
        name="block",
    )(*operands)


def shards(
    query_latent,
    key_latent,
    rotary_key,
    query_gain,
    latent_gain,
    query_content,
    query_rotary,
    key_content,
    value_weight,
    output_weight,
    expert_input,
    norm_gain,
    routes,
    route_weight,
    expert_gate,
    expert_up,
    expert_down,
    shared_gate,
    shared_up,
    shared_down,
):
    group_size = lax.axis_size("tp")
    expert_groups = lax.axis_size("ep")
    token_rows = expert_input.shape[0]
    picks = routes.shape[1]
    local_experts = expert_gate.shape[0]
    expert_total = local_experts * expert_groups
    capacity = 2 * token_rows * picks // expert_total
    if group_size != 4 or capacity % 16 or not fits_kernel(expert_groups, local_experts * capacity):
        return shards_plain(
            query_latent,
            key_latent,
            rotary_key,
            query_gain,
            latent_gain,
            query_content,
            query_rotary,
            key_content,
            value_weight,
            output_weight,
            expert_input,
            norm_gain,
            routes,
            route_weight,
            expert_gate,
            expert_up,
            expert_down,
            shared_gate,
            shared_up,
            shared_down,
        )
    group_rows_count = expert_input.shape[0] * group_size
    positions = lax.axis_index("ep") * group_rows_count + jnp.arange(
        group_rows_count, dtype=jnp.int32
    )
    frequency = rope_base ** (-jnp.arange(ROTARY // 2, dtype=jnp.float32) * 2.0 / ROTARY)
    angles = positions.astype(jnp.float32)[:, None] * jnp.tile(
        jnp.repeat(frequency, 2), 128 // ROTARY
    )[None, :]
    both = block_call(
        expert_groups,
        capacity,
        query_latent,
        key_latent,
        rotary_key.T,
        query_gain[None, :],
        latent_gain[None, :],
        expert_input,
        norm_gain[None, :],
        routes.T,
        route_weight.T,
        jnp.cos(angles),
        jnp.sin(angles),
        query_content,
        query_rotary,
        key_content,
        value_weight,
        output_weight,
        expert_gate,
        expert_up,
        expert_down,
        shared_gate,
        shared_up,
        shared_down,
    )
    return (both[0], both[1])


def solution(mesh):
    in_specs = (
        P(("ep", "tp"), None),
        P(("ep", "tp"), None),
        P(("ep", "tp"), None),
        P(),
        P(),
        P(),
        P(),
        P(),
        P(),
        P("tp", None),
        P(("ep", "tp"), None),
        P(),
        P(("ep", "tp"), None),
        P(("ep", "tp"), None),
        P("ep", None, "tp"),
        P("ep", None, "tp"),
        P("ep", "tp", None),
        P(None, "tp"),
        P(None, "tp"),
        P("tp", None),
    )
    out_specs = (P(("ep", "tp"), None), P(("ep", "tp"), None))
    return jax.shard_map(shards, mesh=mesh, in_specs=in_specs, out_specs=out_specs, check_vma=False)
```

time: 104 us -> 87.1 us (0.84)
  Pallas kernels: 99.7 us -> 82.6 us
    pallas_call x1, Pallas kernels: 99.7 us -> 82.6 us  [block_call(): pl.pallas_call(lambda *refs: block_kernel(ep_count, capacity, *refs), out...]
where the time goes in v1:
time: 87.1 us; the launch traced here: 86.6 us
  Pallas kernels  82.6 us (95%)
  local copies, waits for them, and re-layouts  2.11 us (2%)
  other arithmetic  1.25 us (1%)
    pallas_call x1, Pallas kernels, block_call(): pl.pallas_call(lambda *refs: block_kernel(ep_count, capacity, *refs), out...  82.6 us
    squeeze x1, local copies, waits for them, and re-layouts, shards(): return (both[0], both[1])  1.87 us

profile of v1, /device:TPU:0, one launch (start us, length us, event | category | flops | bytes accessed | tf_op | source)
XLA Modules:
  0.0 86.6 jit_solution(328178604262423491)
XLA Ops:
  0.7 0.1 broadcast_in_dim.16
  0.7 0.1 tile.7
  0.8 0.1 mul.21
  0.9 1.2 %multiply_sine_fusion = (f32[256,128]{1,0:T(8,128)}, f32[256,128]{1,0:T(8,128)}) fusion(f32[128]{0:T(128)S(1)} %mul.21, f32[256]{0:T(256)S(1)} %add_convert_fusion), kind=kLoop, calls=%fused_computation.2 | loop fusion | flops 32768 | bytes 263680 | tf_op jit(solution)/shard_map/sin | solution.py:1163
  2.2 82.6 %block.1 = bf16[2,64,2048]{2,1,0:T(8,128)(2,1)} custom-call(bf16[64,512]{1,0:T(8,128)(2,1)} %refs_0_.1, bf16[64,256]{1,0:T(8,128)(2,1)} %refs_1_.1, bf16[32,64]{1,0:T(8,128)(2,1)} %bitcast.10, f32[1,512]{1,0:T(1,128)} %bitcast.12, f32[1,256]{1,0:T(1,128)} %bitcast.13, bf16[64,2048]{1,0:T(8,128)(2,1)} %refs_5_.1, f32[1,2048]{1,0:T(1,128)} %bitcast.11, ...), custom_call_target="tpu_custom_call" | custom-call | tf_op jit(solution)/shard_map/block/pallas_call | solution.py:1035
  84.7 1.9 %slice_bitcast_fusion = (bf16[64,2048]{1,0:T(8,128)(2,1)}, bf16[64,2048]{1,0:T(8,128)(2,1)}) fusion(bf16[2,64,2048]{2,1,0:T(8,128)(2,1)} %block.1), kind=kLoop, calls=%fused_computation | loop fusion | bytes 1048576 | tf_op jit(solution)/shard_map/squeeze | solution.py:1176
  (3 shorter events, 0.0 us)

commit v2 on v1

--- a/solution.py
+++ b/solution.py
@@ -2,6 +2,7 @@
 
 import jax
 import jax.numpy as jnp
+import numpy as np
 from jax import lax
 from jax.experimental import pallas as pl
 from jax.experimental.pallas import tpu as pltpu
@@ -255,8 +256,7 @@
 
 
 def fits_kernel(ep_count, slot_rows):
-    power = ep_count & (ep_count - 1) == 0
-    return power and ep_count > NEAR and NEAR * slot_rows % 128 == 0
+    return ep_count == 2 * NEAR and NEAR * slot_rows % 128 == 0
 
 
 def flip(place, bits):
@@ -278,7 +278,7 @@
     row, core = head_index // 2, head_index % 2
     for other in ((1 - row) * 2 + core, row * 2 + 1 - core):
         pl.semaphore_signal(barrier, inc=1, device_id=(me, other), device_id_type=MESH)
-    pl.semaphore_wait(barrier, ep_count + 1)
+    return lambda: pl.semaphore_wait(barrier, ep_count + 1)
 
 
 def gated_rows(rows, gate_weight, up_weight):
@@ -341,17 +341,16 @@
 def block_kernel(
     ep_count,
     capacity,
-    query_latent_ref,
-    key_latent_ref,
-    rotary_key_ref,
-    query_gain_ref,
-    latent_gain_ref,
-    expert_input_ref,
-    norm_gain_ref,
-    routes_ref,
-    route_weight_ref,
-    cosine_ref,
-    sine_ref,
+    query_latent_hbm,
+    key_latent_hbm,
+    rotary_key_hbm,
+    query_gain_hbm,
+    latent_gain_hbm,
+    expert_input_hbm,
+    norm_gain_hbm,
+    routes_hbm,
+    route_weight_hbm,
+    frequency_hbm,
     query_content_hbm,
     query_rotary_hbm,
     key_content_hbm,
@@ -363,7 +362,22 @@
     shared_gate_hbm,
     shared_up_hbm,
     shared_down_hbm,
-    both_out,
+    mixer_out,
+    expert_out,
+    query_latent_ref,
+    key_latent_ref,
+    rotary_key_ref,
+    query_gain_ref,
+    latent_gain_ref,
+    expert_input_ref,
+    norm_gain_ref,
+    routes_ref,
+    route_weight_ref,
+    frequency_ref,
+    cosine_ref,
+    sine_ref,
+    mixer_rows,
+    expert_rows,
     slots_ref,
     peer_slots_ref,
     query_columns_ref,
@@ -422,6 +436,8 @@
     side_recv,
     own_sem,
     weight_sem,
+    input_sem,
+    out_sem,
 ):
     me = lax.axis_index("ep")
     head_index = lax.axis_index("tp")
@@ -436,6 +452,27 @@
     picks = routes_ref.shape[0]
     stripe = math.gcd(width, 512)
     far_steps = range(NEAR, ep_count)
+    chunks = ((NEAR + 2, ep_count), (NEAR, NEAR + 2))
+    greeted = greet(ep_count, me, head_index)
+    arguments = [
+        pltpu.make_async_copy(source, target, input_sem.at[place])
+        for place, (source, target) in enumerate(
+            (
+                (key_latent_hbm, key_latent_ref),
+                (rotary_key_hbm, rotary_key_ref),
+                (latent_gain_hbm, latent_gain_ref),
+                (frequency_hbm, frequency_ref),
+                (expert_input_hbm, expert_input_ref),
+                (norm_gain_hbm, norm_gain_ref),
+                (routes_hbm, routes_ref),
+                (route_weight_hbm, route_weight_ref),
+                (query_latent_hbm, query_latent_ref),
+                (query_gain_hbm, query_gain_ref),
+            )
+        )
+    ]
+    for argument in arguments:
+        argument.start()
     near_place = me % NEAR
 
     def peer(step):
@@ -487,6 +524,12 @@
         )
         return narrow(entries * cosine + crossed * sine)
 
+    def angles(first, count):
+        places = first + lax.broadcasted_iota(jnp.int32, (count, 128), 0)
+        return places.astype(jnp.float32) * frequency_ref[...]
+
+    for argument in arguments[:4]:
+        argument.wait()
     rank_width = key_latent_ref.shape[1]
     latents[core, 0, :, :rank_width] = narrow(rms_rows(key_latent_ref[...], latent_gain_ref[...]))
     repeats = narrow(
@@ -497,7 +540,7 @@
             0.0,
         )
     )
-    own_span = pl.ds(pl.multiple_of(head_index * own_rows, own_rows), own_rows)
+    own_angles = angles((me * 4 + head_index) * own_rows, own_rows)
     latents[core, 0, :, rank_width:] = turn(
         lax.dot_general(
             rotary_key_ref[...],
@@ -505,14 +548,18 @@
             (((0,), (0,)), ((), ())),
             preferred_element_type=jnp.float32,
         ),
-        cosine_ref[own_span, :],
-        sine_ref[own_span, :],
-    )
+        jnp.cos(own_angles),
+        jnp.sin(own_angles),
+    )
+    for argument in arguments[4:]:
+        argument.wait()
+    expert_normed = narrow(rms_rows(expert_input_ref[...], norm_gain_ref[...]))
+    tokens[row, core] = expert_normed
     queries[row, core] = narrow(rms_rows(query_latent_ref[...], query_gain_ref[...]))
     info_ref[...] = jnp.zeros(info_ref.shape, jnp.float32)
     info_ref[:picks, :own_rows] = routes_ref[...].astype(jnp.float32)
     info_ref[picks : 2 * picks, :own_rows] = route_weight_ref[...]
-    greet(ep_count, me, head_index)
+    greeted()
 
     def latent_ep(step):
         if step % 2 == 0:
@@ -567,7 +614,10 @@
     def moved_rows(step, route):
         origin_row, send_sem, recv_sem, device = routes_of[route]
         block = rows.at[origin_row, core, step]
-        return remote(block, block, send_sem.at[0, step], recv_sem.at[0, step], device)
+        source = block
+        if step == 0:
+            source = peer_slots_ref.at[near_place] if route == "cross" else slots_ref.at[me]
+        return remote(source, block, send_sem.at[0, step], recv_sem.at[0, step], device)
 
     def moved(buffer, place, route):
         origin_row, send_sem, recv_sem, device = routes_of[route]
@@ -585,11 +635,9 @@
     latent_core(0).start()
     info_y.start()
     for route in ("y", "core"):
+        moved(tokens, 0, route).start()
+    for route in ("y", "core"):
         moved(queries, 1, route).start()
-    expert_normed = narrow(rms_rows(expert_input_ref[...], norm_gain_ref[...]))
-    tokens[row, core] = expert_normed
-    for route in ("y", "core"):
-        moved(tokens, 0, route).start()
     expert_total = local_experts * ep_count
     picker, weight = choose_slots(
         routes_ref[...].T, route_weight_ref[...].T, expert_total, capacity, 0, ep_count * slot_rows
@@ -607,12 +655,14 @@
             ).reshape(target.shape[0], slot_rows, stripe)
 
     fill(slots_ref, picker, row)
-    for step in range(1, ep_count):
+    for step in (6, 7, 1, 2, 3):
         slots_ep(step).start()
     own_slots = pltpu.make_async_copy(slots_ref.at[me], rows.at[row, core, 0], own_sem.at[0])
     own_slots.start()
-    own_slots.wait()
     moved_rows(0, "core").start()
+    group_angles = angles(me * group_rows, group_rows)
+    cosine_ref[...] = jnp.cos(group_angles)
+    sine_ref[...] = jnp.sin(group_angles)
 
     def pass_latents(steps):
         for step in steps:
@@ -621,9 +671,6 @@
                 latent_ep(step + 1).start()
             latent_core(step).start()
 
-    pass_latents(range(2, ep_count, 2))
-    moved(queries, 1, "y").wait_recv()
-    moved(queries, 1, "cross").start()
     info_y.wait_recv()
     peer_picker, peer_weight = choose_slots(
         peer_info_ref[:picks, :own_rows].T.astype(jnp.int32),
@@ -634,17 +681,21 @@
         NEAR * slot_rows,
     )
     store_split(peer_weight_ref, peer_weight)
+    pass_latents(range(2, ep_count, 2))
     moved(tokens, 0, "y").wait_recv()
     moved(tokens, 0, "cross").start()
     fill(peer_slots_ref, peer_picker, 1 - row)
     for step in range(1, NEAR):
         peer_slots_ep(step).start()
+    for step in (4, 5):
+        slots_ep(step).start()
     peer_own = pltpu.make_async_copy(
         peer_slots_ref.at[near_place], rows.at[1 - row, core, 0], own_sem.at[1]
     )
     peer_own.start()
-    peer_own.wait()
     moved_rows(0, "cross").start()
+    moved(queries, 1, "y").wait_recv()
+    moved(queries, 1, "cross").start()
     pass_latents(range(1, ep_count, 2))
     for route in ("core", "cross"):
         moved(queries, 1, route).wait_recv()
@@ -791,37 +842,6 @@
             peer_slots_ep(step).wait_recv()
         moved_rows(step, "cross").start()
 
-    project()
-    arrive(1)
-    attend(1, 0)
-    arrive(2)
-    arrive(3)
-    attend(1, 1)
-    sum_y.start()
-    arrive(4)
-    attend(0, 0)
-    arrive(5)
-    arrive_peer(1)
-    arrive_peer(4)
-    attend(0, 1)
-    arrive(6)
-    arrive_peer(5)
-    merge()
-    mix()
-    mixed_half.start()
-    for step in range(7, ep_count):
-        arrive(step)
-    arrive_peer(2)
-    arrive_peer(3)
-    share()
-    shared_half.start()
-    for step in range(6, ep_count):
-        arrive_peer(step)
-    mixed_far()
-
-    for fetch in fetches[12:]:
-        fetch.wait()
-
     def spans(expert):
         return slice(expert * capacity, (expert + 1) * capacity)
 
@@ -845,17 +865,18 @@
         return remote(
             part.at[:, 1 - core, :NEAR],
             half_rows.at[:, :NEAR],
-            half_send.at[local_experts],
-            half_recv.at[local_experts],
+            half_send.at[2, 0],
+            half_recv.at[2, 0],
             core_peer,
         )
 
-    def far_half(expert):
+    def far_half(chunk, expert):
+        first, last = chunks[chunk]
         return remote(
-            part.at[:, 1 - core, NEAR:, spans(expert)],
-            half_rows.at[:, NEAR:, spans(expert)],
-            half_send.at[expert],
-            half_recv.at[expert],
+            part.at[:, 1 - core, first:last, spans(expert)],
+            half_rows.at[:, first:last, spans(expert)],
+            half_send.at[chunk, expert],
+            half_recv.at[chunk, expert],
             core_peer,
         )
 
@@ -897,13 +918,15 @@
 
     def settle_near():
         near_half().wait_recv()
-        for step in list(range(1, NEAR)) + [0]:
+        order = list(range(1, NEAR)) + [0]
+        for step in order:
             outer = narrow(wide(part[1 - row, core, step]) + wide(half_rows[1 - row, step]))
             if step:
                 part[1 - row, core, step] = outer
                 back_peer(step).start()
             else:
                 returned_peer[near_place] = outer
+        for step in order:
             total = narrow(wide(part[row, core, step]) + wide(half_rows[row, step]))
             if step:
                 part[row, core, step] = total
@@ -911,18 +934,18 @@
             else:
                 returned[me] = total
 
-    def settle_outer(expert):
-        far_half(expert).wait_recv()
+    def settle_outer(chunk, expert):
+        far_half(chunk, expert).wait_recv()
         span = spans(expert)
-        for step in far_steps:
+        for step in range(*chunks[chunk]):
             part[1 - row, core, step, span] = narrow(
                 wide(part[1 - row, core, step, span]) + wide(half_rows[1 - row, step, span])
             )
             y_copy(step, expert).start()
 
-    def settle_far(expert):
+    def settle_far(chunk, expert):
         span = spans(expert)
-        for step in far_steps:
+        for step in range(*chunks[chunk]):
             y_copy(step, expert).wait_recv()
             part[row, core, step, span] = narrow(
                 wide(part[row, core, step, span])
@@ -936,19 +959,63 @@
             for route in ("core", "cross"):
                 moved_rows(step, route).wait_recv()
 
+    def far_chunk(chunk):
+        wait_rows(range(*chunks[chunk]))
+        for expert in range(local_experts):
+            compute(*chunks[chunk], expert)
+            far_half(chunk, expert).start()
+
+    project()
+    attend(1, 0)
+    attend(1, 1)
+    sum_y.start()
+    arrive(6)
+    arrive(7)
+    attend(0, 0)
+    for step in range(1, NEAR):
+        arrive(step)
+    arrive_peer(1)
+    attend(0, 1)
+    arrive_peer(6)
+    arrive_peer(7)
+    merge()
+    mix()
+    mixed_half.start()
+    for fetch in fetches[12:]:
+        fetch.wait()
+    far_chunk(0)
+    share()
+    shared_half.start()
+    for expert in range(local_experts):
+        settle_outer(0, expert)
+    mixed_far()
+    arrive(4)
+    settle_far(0, 0)
+    arrive(5)
+    for expert in range(1, local_experts):
+        settle_far(0, expert)
+    arrive_peer(2)
+    arrive_peer(3)
+    arrive_peer(4)
+    own_slots.wait()
+    peer_own.wait()
     wait_rows(range(NEAR))
     for expert in range(local_experts):
         compute(0, NEAR, expert)
     near_half().start()
-    wait_rows(far_steps)
+    arrive_peer(5)
+    far_chunk(1)
+    settle_near()
     for expert in range(local_experts):
-        compute(NEAR, ep_count, expert)
-        far_half(expert).start()
-        if expert == 0:
-            settle_near()
-        else:
-            settle_outer(expert - 1)
-    settle_outer(local_experts - 1)
+        settle_outer(1, expert)
+    for expert in range(local_experts):
+        settle_far(1, expert)
+    mixed_y.wait_recv()
+    mixer_rows[...] = narrow(
+        wide(mixed[row, core]) + wide(half_mixed[row]) + wide(far_mixed[...])
+    )
+    mixer_copy = pltpu.make_async_copy(mixer_rows, mixer_out, out_sem.at[0])
+    mixer_copy.start()
     for step in range(1, NEAR):
         back_peer(step).wait_recv()
     shared_half.wait_recv()
@@ -963,19 +1030,17 @@
             + wide(half_shared[1 - row, :, cut])
         )
     shared_y.start()
-    for expert in range(local_experts):
-        settle_far(expert)
-    mixed_y.wait_recv()
-    both_out[0] = narrow(wide(mixed[row, core]) + wide(half_mixed[row]) + wide(far_mixed[...]))
-    shared_y.wait_recv()
     for step in range(1, NEAR):
         back_near(step).wait_recv()
-    for expert in range(local_experts):
-        for step in far_steps:
-            back_far(step, expert).wait_recv()
-    for start in range(0, width, stripe):
+    for chunk in range(2):
+        for expert in range(local_experts):
+            for step in range(*chunks[chunk]):
+                back_far(step, expert).wait_recv()
+    shared_y.wait_recv()
+    out_copies = []
+    for place, start in enumerate(range(0, width, stripe)):
         cut = slice(start, start + stripe)
-        both_out[1, :, cut] = narrow(
+        expert_rows[:, cut] = narrow(
             weighted_rows(
                 weight_ref[...], returned[:, :, cut].reshape(ep_count * slot_rows, stripe)
             )
@@ -983,6 +1048,12 @@
             + wide(half_shared[row, :, cut])
             + wide(far_shared[:, cut])
         )
+        out_copies.append(
+            pltpu.make_async_copy(
+                expert_rows.at[:, cut], expert_out.at[:, cut], out_sem.at[1 + place]
+            )
+        )
+        out_copies[-1].start()
 
     for step in range(1, ep_count):
         latent_ep(step).wait_send()
@@ -1003,20 +1074,22 @@
     for route in ("y", "core", "cross"):
         moved(queries, 1, route).wait_send()
         moved(tokens, 0, route).wait_send()
-    for expert in range(local_experts):
-        far_half(expert).wait_send()
+    for chunk in range(2):
+        for expert in range(local_experts):
+            far_half(chunk, expert).wait_send()
     for copy in (info_y, sum_y, near_half(), shared_half, mixed_half, shared_y, mixed_y):
         copy.wait_send()
+    for copy in [mixer_copy] + out_copies:
+        copy.wait()
 
 
 def block_call(ep_count, capacity, *operands):
     query_latent, key_latent = operands[:2]
     own_rows, width = operands[5].shape
-    head_lanes = operands[15].shape[0]
-    local_experts = operands[16].shape[0]
+    head_lanes = operands[14].shape[0]
+    local_experts = operands[15].shape[0]
     slot_rows = local_experts * capacity
     latent_shape = (own_rows, key_latent.shape[1] + 128)
-    vmem = pl.BlockSpec(memory_space=pltpu.VMEM)
     anywhere = pl.BlockSpec(memory_space=pl.ANY)
 
     def held(*shape):
@@ -1034,10 +1107,15 @@
     side = (own_rows, width)
     return pl.pallas_call(
         lambda *refs: block_kernel(ep_count, capacity, *refs),
-        out_shape=jax.ShapeDtypeStruct((2, own_rows, width), jnp.bfloat16),
-        in_specs=[vmem] * 11 + [anywhere] * 11,
-        out_specs=vmem,
-        scratch_shapes=[
+        out_shape=[jax.ShapeDtypeStruct(side, jnp.bfloat16)] * 2,
+        in_specs=[anywhere] * 21,
+        out_specs=[anywhere] * 2,
+        scratch_shapes=[pltpu.VMEM(operand.shape, operand.dtype) for operand in operands[:10]]
+        + [
+            precise(group_rows, 128),
+            precise(group_rows, 128),
+            held(*side),
+            held(*side),
             held(ep_count, *row_block),
             held(NEAR, *row_block),
             held(2, query_latent.shape[1], head_lanes + 128),
@@ -1050,7 +1128,7 @@
             held(2, 2, *side),
             held(2, 2, *query_latent.shape),
         ]
-        + [held(*operand.shape) for operand in operands[16:]]
+        + [held(*operand.shape) for operand in operands[15:]]
         + [
             held(2, key_rows, head_lanes + 128),
             held(2, key_rows, head_lanes),
@@ -1077,9 +1155,9 @@
         + [sems(2, ep_count + 1)] * 8
         + [sems(2, NEAR)] * 2
         + [sems(local_experts, ep_count)] * 4
-        + [sems(local_experts + 1)] * 2
+        + [sems(3, local_experts)] * 2
         + [sems(4)] * 2
-        + [sems(2), sems(15)],
+        + [sems(2), sems(15), sems(10), sems(1 + width // math.gcd(width, 512))],
         compiler_params=pltpu.CompilerParams(
             collective_id=0, has_side_effects=True, vmem_limit_bytes=VMEM_LIMIT
         ),
@@ -1139,15 +1217,8 @@
             shared_up,
             shared_down,
         )
-    group_rows_count = expert_input.shape[0] * group_size
-    positions = lax.axis_index("ep") * group_rows_count + jnp.arange(
-        group_rows_count, dtype=jnp.int32
-    )
-    frequency = rope_base ** (-jnp.arange(ROTARY // 2, dtype=jnp.float32) * 2.0 / ROTARY)
-    angles = positions.astype(jnp.float32)[:, None] * jnp.tile(
-        jnp.repeat(frequency, 2), 128 // ROTARY
-    )[None, :]
-    both = block_call(
+    frequency = rope_base ** (-np.arange(ROTARY // 2) * 2.0 / ROTARY)
+    return block_call(
         expert_groups,
         capacity,
         query_latent,
@@ -1159,8 +1230,7 @@
         norm_gain[None, :],
         routes.T,
         route_weight.T,
-        jnp.cos(angles),
-        jnp.sin(angles),
+        jnp.asarray(np.tile(np.repeat(frequency, 2), 128 // ROTARY)[None, :], jnp.float32),
         query_content,
         query_rotary,
         key_content,
@@ -1173,7 +1243,6 @@
         shared_up,
         shared_down,
     )
-    return (both[0], both[1])
 
 
 def solution(mesh):

time: 87.1 us -> 95.2 us (1.093)
  Pallas kernels: 82.6 us -> 90.9 us
  other arithmetic: 1.25 us -> 0 us
  local copies, waits for them, and re-layouts: 2.11 us -> 3.34 us
    pallas_call x1, Pallas kernels: 82.6 us -> 90.9 us  [block_call(): pl.pallas_call(lambda *refs: block_kernel(ep_count, capacity, *refs), out...]
    unnamed x0 -> x2, local copies, waits for them, and re-layouts: none -> 3.34 us
    squeeze x1 -> x0, local copies, waits for them, and re-layouts: 1.87 us -> none  [shards(): return (both[0], both[1])]
    sin x1 -> x0, other arithmetic: 1.24 us -> none  [shards(): jnp.sin(angles)]
where the time goes in v2:
time: 95.2 us; the launch traced here: 94.9 us
  Pallas kernels  90.9 us (95%)
  local copies, waits for them, and re-layouts  3.34 us (4%)
    pallas_call x1, Pallas kernels, block_call(): pl.pallas_call(lambda *refs: block_kernel(ep_count, capacity, *refs), out...  90.9 us
    unnamed x2, local copies, waits for them, and re-layouts  3.34 us

profile of v2, /device:TPU:0, one launch (start us, length us, event | category | flops | bytes accessed | tf_op | source)
XLA Modules:
  0.0 94.9 jit_solution(11742298472664146897)
XLA Ops:
  0.6 90.9 %block.1 = (bf16[64,2048]{1,0:T(8,128)(2,1)}, bf16[64,2048]{1,0:T(8,128)(2,1)}) custom-call(bf16[64,512]{1,0:T(8,128)(2,1)} %refs_0_.1, bf16[64,256]{1,0:T(8,128)(2,1)} %refs_1_.1, bf16[32,64]{1,0:T(8,128)(2,1)} %bitcast.6, f32[1,512]{1,0:T(1,128)} %bitcast.8, f32[1,256]{1,0:T(1,128)} %bitcast.9, bf16[64,2048]{1,0:T(8,128)(2,1)} %refs_5_.1, ...), custom_call_target="tpu_custom_call" | custom-call | tf_op jit(solution)/shard_map/block/pallas_call | solution.py:1108
  91.5 1.7 %copy.25 = bf16[64,2048]{1,0:T(8,128)(2,1)} copy(bf16[64,2048]{1,0:T(8,128)(2,1)} %get-tuple-element.4) | data formatting | bytes 524288
  93.2 1.7 %copy.26 = bf16[64,2048]{1,0:T(8,128)(2,1)} copy(bf16[64,2048]{1,0:T(8,128)(2,1)} %get-tuple-element.5) | data formatting | bytes 524288

commit v3 on v2

--- a/solution.py
+++ b/solution.py
@@ -259,13 +259,11 @@
     return ep_count == 2 * NEAR and NEAR * slot_rows % 128 == 0
 
 
-def flip(place, bits):
+def flip(place, bits, width=3):
     flipped = place
-    bit = 1
-    while bit <= bits:
-        if bits & bit:
-            flipped = flipped + bit * (1 - 2 * (place // bit % 2))
-        bit *= 2
+    for power in range(width):
+        bit = 2**power
+        flipped = flipped + bit * (bits // bit % 2) * (1 - 2 * (place // bit % 2))
     return flipped
 
 
@@ -362,8 +360,7 @@
     shared_gate_hbm,
     shared_up_hbm,
     shared_down_hbm,
-    mixer_out,
-    expert_out,
+    both_out,
     query_latent_ref,
     key_latent_ref,
     rotary_key_ref,
@@ -376,8 +373,6 @@
     frequency_ref,
     cosine_ref,
     sine_ref,
-    mixer_rows,
-    expert_rows,
     slots_ref,
     peer_slots_ref,
     query_columns_ref,
@@ -437,7 +432,6 @@
     own_sem,
     weight_sem,
     input_sem,
-    out_sem,
 ):
     me = lax.axis_index("ep")
     head_index = lax.axis_index("tp")
@@ -452,7 +446,8 @@
     picks = routes_ref.shape[0]
     stripe = math.gcd(width, 512)
     far_steps = range(NEAR, ep_count)
-    chunks = ((NEAR + 2, ep_count), (NEAR, NEAR + 2))
+    outermost = 1 - (me // 2 + me // 4) % 2
+    chunks = (NEAR + 2 * (1 - outermost), NEAR + 2 * outermost)
     greeted = greet(ep_count, me, head_index)
     arguments = [
         pltpu.make_async_copy(source, target, input_sem.at[place])
@@ -615,7 +610,7 @@
         origin_row, send_sem, recv_sem, device = routes_of[route]
         block = rows.at[origin_row, core, step]
         source = block
-        if step == 0:
+        if isinstance(step, int) and step == 0:
             source = peer_slots_ref.at[near_place] if route == "cross" else slots_ref.at[me]
         return remote(source, block, send_sem.at[0, step], recv_sem.at[0, step], device)
 
@@ -629,9 +624,8 @@
     info_y = remote(
         info_ref, peer_info_ref, y_send.at[0, 0], y_recv.at[0, 0], y_peer
     )
-    for step in range(1, ep_count):
-        if step == 1 or step % 2 == 0:
-            latent_ep(step).start()
+    for step in (6, 4, 2, 1):
+        latent_ep(step).start()
     latent_core(0).start()
     info_y.start()
     for route in ("y", "core"):
@@ -655,7 +649,12 @@
             ).reshape(target.shape[0], slot_rows, stripe)
 
     fill(slots_ref, picker, row)
-    for step in (6, 7, 1, 2, 3):
+    @pl.when(outermost == 0)
+    def _():
+        for step in (6, 4, 7, 5):
+            slots_ep(step).start()
+
+    for step in (2, 3):
         slots_ep(step).start()
     own_slots = pltpu.make_async_copy(slots_ref.at[me], rows.at[row, core, 0], own_sem.at[0])
     own_slots.start()
@@ -682,26 +681,17 @@
     )
     store_split(peer_weight_ref, peer_weight)
     pass_latents(range(2, ep_count, 2))
+    slots_ep(1).start()
     moved(tokens, 0, "y").wait_recv()
     moved(tokens, 0, "cross").start()
     fill(peer_slots_ref, peer_picker, 1 - row)
     for step in range(1, NEAR):
         peer_slots_ep(step).start()
-    for step in (4, 5):
-        slots_ep(step).start()
     peer_own = pltpu.make_async_copy(
         peer_slots_ref.at[near_place], rows.at[1 - row, core, 0], own_sem.at[1]
     )
     peer_own.start()
     moved_rows(0, "cross").start()
-    moved(queries, 1, "y").wait_recv()
-    moved(queries, 1, "cross").start()
-    pass_latents(range(1, ep_count, 2))
-    for route in ("core", "cross"):
-        moved(queries, 1, route).wait_recv()
-    for step in range(ep_count):
-        latent_core(step).wait_recv()
-
     def project():
         for fetch in fetches[:8]:
             fetch.wait()
@@ -831,23 +821,29 @@
 
     def arrive(step):
         slots_ep(step).wait_recv()
-        if step >= NEAR:
-            moved_rows(step, "y").start()
         moved_rows(step, "core").start()
 
     def arrive_peer(step):
-        if step >= NEAR:
-            moved_rows(step, "y").wait_recv()
-        else:
-            peer_slots_ep(step).wait_recv()
+        peer_slots_ep(step).wait_recv()
+        moved_rows(step, "cross").start()
+
+    def arrive_far(chunk, place):
+        step = chunks[chunk] + place
+        slots_ep(step).wait_recv()
+        moved_rows(step, "y").start()
+        moved_rows(step, "core").start()
+
+    def arrive_far_peer(chunk, place):
+        step = chunks[chunk] + place
+        moved_rows(step, "y").wait_recv()
         moved_rows(step, "cross").start()
 
     def spans(expert):
         return slice(expert * capacity, (expert + 1) * capacity)
 
-    def compute(first, last, expert):
+    def compute(first, count, expert):
         span = spans(expert)
-        block = rows[:, :, first:last, span, :].reshape(4 * (last - first) * capacity, width)
+        block = rows[:, :, pl.ds(first, count), span, :].reshape(4 * count * capacity, width)
         hidden = gated_rows(block, gate_ref[expert], up_ref[expert])
         for start in range(0, width, stripe):
             product = narrow(
@@ -857,8 +853,8 @@
                     preferred_element_type=jnp.float32,
                 )
             )
-            part[:, :, first:last, span, start : start + stripe] = product.reshape(
-                2, 2, last - first, capacity, stripe
+            part[:, :, pl.ds(first, count), span, start : start + stripe] = product.reshape(
+                2, 2, count, capacity, stripe
             )
 
     def near_half():
@@ -871,10 +867,10 @@
         )
 
     def far_half(chunk, expert):
-        first, last = chunks[chunk]
+        steps = pl.ds(chunks[chunk], 2)
         return remote(
-            part.at[:, 1 - core, first:last, spans(expert)],
-            half_rows.at[:, first:last, spans(expert)],
+            part.at[:, 1 - core, steps, spans(expert)],
+            half_rows.at[:, steps, spans(expert)],
             half_send.at[chunk, expert],
             half_recv.at[chunk, expert],
             core_peer,
@@ -937,7 +933,7 @@
     def settle_outer(chunk, expert):
         far_half(chunk, expert).wait_recv()
         span = spans(expert)
-        for step in range(*chunks[chunk]):
+        for step in (chunks[chunk], chunks[chunk] + 1):
             part[1 - row, core, step, span] = narrow(
                 wide(part[1 - row, core, step, span]) + wide(half_rows[1 - row, step, span])
             )
@@ -945,7 +941,7 @@
 
     def settle_far(chunk, expert):
         span = spans(expert)
-        for step in range(*chunks[chunk]):
+        for step in (chunks[chunk], chunks[chunk] + 1):
             y_copy(step, expert).wait_recv()
             part[row, core, step, span] = narrow(
                 wide(part[row, core, step, span])
@@ -960,62 +956,92 @@
                 moved_rows(step, route).wait_recv()
 
     def far_chunk(chunk):
-        wait_rows(range(*chunks[chunk]))
+        wait_rows((chunks[chunk], chunks[chunk] + 1))
         for expert in range(local_experts):
-            compute(*chunks[chunk], expert)
+            compute(chunks[chunk], 2, expert)
             far_half(chunk, expert).start()
 
-    project()
-    attend(1, 0)
-    attend(1, 1)
-    sum_y.start()
-    arrive(6)
-    arrive(7)
-    attend(0, 0)
+    def gather_latents():
+        moved(queries, 1, "y").wait_recv()
+        moved(queries, 1, "cross").start()
+        pass_latents(range(1, ep_count, 2))
+
+    def finish_latents():
+        for route in ("core", "cross"):
+            moved(queries, 1, route).wait_recv()
+        for step in range(ep_count):
+            latent_core(step).wait_recv()
+
+    def near_compute():
+        own_slots.wait()
+        peer_own.wait()
+        wait_rows(range(NEAR))
+        for expert in range(local_experts):
+            compute(0, NEAR, expert)
+        near_half().start()
+
+    def inner(work):
+        pl.when(outermost == 0)(work)
+
+    def outer(work):
+        pl.when(outermost == 1)(work)
+
+    def attend_peer():
+        gather_latents()
+        finish_latents()
+        project()
+        attend(1, 0)
+        attend(1, 1)
+        sum_y.start()
+
+    def attend_own():
+        attend(0, 0)
+        attend(0, 1)
+        merge()
+        mix()
+        mixed_half.start()
+
+    def send_far():
+        for step in (6, 4, 7, 5):
+            slots_ep(step).start()
+
+    arrive_far(0, 0)
+    outer(attend_peer)
+    arrive_far(0, 1)
+    outer(send_far)
+    outer(attend_own)
+    for fetch in fetches[12:]:
+        fetch.wait()
+    for place in range(2):
+        arrive_far_peer(0, place)
+    far_chunk(0)
     for step in range(1, NEAR):
         arrive(step)
-    arrive_peer(1)
-    attend(0, 1)
-    arrive_peer(6)
-    arrive_peer(7)
-    merge()
-    mix()
-    mixed_half.start()
-    for fetch in fetches[12:]:
-        fetch.wait()
-    far_chunk(0)
+    for expert in range(local_experts):
+        settle_outer(0, expert)
+    for step in range(1, NEAR):
+        arrive_peer(step)
+    inner(attend_peer)
+    inner(near_compute)
+    arrive_far(1, 0)
+    arrive_far(1, 1)
+    outer(near_compute)
+    settle_far(0, 0)
+    settle_far(0, 1)
+    settle_near()
+    inner(attend_own)
     share()
     shared_half.start()
-    for expert in range(local_experts):
-        settle_outer(0, expert)
+    for place in range(2):
+        arrive_far_peer(1, place)
     mixed_far()
-    arrive(4)
-    settle_far(0, 0)
-    arrive(5)
-    for expert in range(1, local_experts):
-        settle_far(0, expert)
-    arrive_peer(2)
-    arrive_peer(3)
-    arrive_peer(4)
-    own_slots.wait()
-    peer_own.wait()
-    wait_rows(range(NEAR))
-    for expert in range(local_experts):
-        compute(0, NEAR, expert)
-    near_half().start()
-    arrive_peer(5)
     far_chunk(1)
-    settle_near()
     for expert in range(local_experts):
         settle_outer(1, expert)
     for expert in range(local_experts):
         settle_far(1, expert)
     mixed_y.wait_recv()
-    mixer_rows[...] = narrow(
-        wide(mixed[row, core]) + wide(half_mixed[row]) + wide(far_mixed[...])
-    )
-    mixer_copy = pltpu.make_async_copy(mixer_rows, mixer_out, out_sem.at[0])
-    mixer_copy.start()
+    both_out[0] = narrow(wide(mixed[row, core]) + wide(half_mixed[row]) + wide(far_mixed[...]))
     for step in range(1, NEAR):
         back_peer(step).wait_recv()
     shared_half.wait_recv()
@@ -1032,15 +1058,13 @@
     shared_y.start()
     for step in range(1, NEAR):
         back_near(step).wait_recv()
-    for chunk in range(2):
+    for step in far_steps:
         for expert in range(local_experts):
-            for step in range(*chunks[chunk]):
-                back_far(step, expert).wait_recv()
+            back_far(step, expert).wait_recv()
     shared_y.wait_recv()
-    out_copies = []
-    for place, start in enumerate(range(0, width, stripe)):
+    for start in range(0, width, stripe):
         cut = slice(start, start + stripe)
-        expert_rows[:, cut] = narrow(
+        both_out[1, :, cut] = narrow(
             weighted_rows(
                 weight_ref[...], returned[:, :, cut].reshape(ep_count * slot_rows, stripe)
             )
@@ -1048,12 +1072,6 @@
             + wide(half_shared[row, :, cut])
             + wide(far_shared[:, cut])
         )
-        out_copies.append(
-            pltpu.make_async_copy(
-                expert_rows.at[:, cut], expert_out.at[:, cut], out_sem.at[1 + place]
-            )
-        )
-        out_copies[-1].start()
 
     for step in range(1, ep_count):
         latent_ep(step).wait_send()
@@ -1079,8 +1097,6 @@
             far_half(chunk, expert).wait_send()
     for copy in (info_y, sum_y, near_half(), shared_half, mixed_half, shared_y, mixed_y):
         copy.wait_send()
-    for copy in [mixer_copy] + out_copies:
-        copy.wait()
 
 
 def block_call(ep_count, capacity, *operands):
@@ -1107,15 +1123,13 @@
     side = (own_rows, width)
     return pl.pallas_call(
         lambda *refs: block_kernel(ep_count, capacity, *refs),
-        out_shape=[jax.ShapeDtypeStruct(side, jnp.bfloat16)] * 2,
+        out_shape=jax.ShapeDtypeStruct((2,) + side, jnp.bfloat16),
         in_specs=[anywhere] * 21,
-        out_specs=[anywhere] * 2,
+        out_specs=pl.BlockSpec(memory_space=pltpu.VMEM),
         scratch_shapes=[pltpu.VMEM(operand.shape, operand.dtype) for operand in operands[:10]]
         + [
             precise(group_rows, 128),
             precise(group_rows, 128),
-            held(*side),
-            held(*side),
             held(ep_count, *row_block),
             held(NEAR, *row_block),
             held(2, query_latent.shape[1], head_lanes + 128),
@@ -1157,7 +1171,7 @@
         + [sems(local_experts, ep_count)] * 4
         + [sems(3, local_experts)] * 2
         + [sems(4)] * 2
-        + [sems(2), sems(15), sems(10), sems(1 + width // math.gcd(width, 512))],
+        + [sems(2), sems(15), sems(10)],
         compiler_params=pltpu.CompilerParams(
             collective_id=0, has_side_effects=True, vmem_limit_bytes=VMEM_LIMIT
         ),
@@ -1218,7 +1232,7 @@
             shared_down,
         )
     frequency = rope_base ** (-np.arange(ROTARY // 2) * 2.0 / ROTARY)
-    return block_call(
+    both = block_call(
         expert_groups,
         capacity,
         query_latent,
@@ -1243,6 +1257,7 @@
         shared_up,
         shared_down,
     )
+    return (both[0], both[1])
 
 
 def solution(mesh):

time: 95.2 us -> 74.6 us (0.78)
  Pallas kernels: 90.9 us -> 71.9 us
  local copies, waits for them, and re-layouts: 3.34 us -> 1.87 us
    pallas_call x1, Pallas kernels: 90.9 us -> 71.9 us  [block_call(): pl.pallas_call(lambda *refs: block_kernel(ep_count, capacity, *refs), out...]
    unnamed x2 -> x0, local copies, waits for them, and re-layouts: 3.34 us -> none
    squeeze x0 -> x1, local copies, waits for them, and re-layouts: none -> 1.87 us  [shards(): return (both[0], both[1])]
where the time goes in v3:
time: 74.6 us; the launch traced here: 74.4 us
  Pallas kernels  71.9 us (96%)
  local copies, waits for them, and re-layouts  1.87 us (3%)
    pallas_call x1, Pallas kernels, block_call(): pl.pallas_call(lambda *refs: block_kernel(ep_count, capacity, *refs), out...  71.9 us
    squeeze x1, local copies, waits for them, and re-layouts, shards(): return (both[0], both[1])  1.87 us

profile of v3, /device:TPU:0, one launch (start us, length us, event | category | flops | bytes accessed | tf_op | source)
XLA Modules:
  0.0 74.4 jit_solution(8932059232456578085)
XLA Ops:
  0.6 71.9 %block.1 = bf16[2,64,2048]{2,1,0:T(8,128)(2,1)} custom-call(bf16[64,512]{1,0:T(8,128)(2,1)} %refs_0_.1, bf16[64,256]{1,0:T(8,128)(2,1)} %refs_1_.1, bf16[32,64]{1,0:T(8,128)(2,1)} %bitcast.10, f32[1,512]{1,0:T(1,128)} %bitcast.12, f32[1,256]{1,0:T(1,128)} %bitcast.13, bf16[64,2048]{1,0:T(8,128)(2,1)} %refs_5_.1, f32[1,2048]{1,0:T(1,128)} %bitcast.11, ...), custom_call_target="tpu_custom_call" | custom-call | tf_op jit(solution)/shard_map/block/pallas_call | solution.py:1124
  72.6 1.9 %slice_bitcast_fusion = (bf16[64,2048]{1,0:T(8,128)(2,1)}, bf16[64,2048]{1,0:T(8,128)(2,1)}) fusion(bf16[2,64,2048]{2,1,0:T(8,128)(2,1)} %block.1), kind=kLoop, calls=%fused_computation | loop fusion | bytes 1048576 | tf_op jit(solution)/shard_map/squeeze | solution.py:1260

commit v4 on v3

--- a/solution.py
+++ b/solution.py
@@ -411,6 +411,8 @@
     own_stats,
     sent_sum,
     far_sum,
+    sent_stats,
+    far_stats,
     ep_send,
     ep_recv,
     y_send,
@@ -506,7 +508,9 @@
         (down_hbm, down_ref),
     ]
     fetches = [
-        pltpu.make_async_copy(source, target, weight_sem.at[place])
+        pltpu.make_async_copy(
+            source, target, weight_sem.at[place % 4 // 2 if place < 8 else place - 6]
+        )
         for place, (source, target) in enumerate(fetch_list)
     ]
     for fetch in fetches:
@@ -561,14 +565,14 @@
             return remote(
                 latents.at[core, 0],
                 latents.at[core, step],
-                ep_send.at[1, step],
+                ep_send.at[1],
                 ep_recv.at[1, step],
                 peer(step),
             )
         return remote(
             latents.at[core, step - 1],
             latents.at[core, step],
-            ep_send.at[1, step],
+            ep_send.at[1],
             ep_recv.at[1, step],
             peer(1),
         )
@@ -577,8 +581,8 @@
         return remote(
             latents.at[core, step],
             latents.at[core, step],
-            core_send.at[1, step],
-            core_recv.at[1, step],
+            core_send.at[1],
+            core_recv.at[1],
             core_peer,
         )
 
@@ -586,7 +590,7 @@
         return remote(
             slots_ref.at[flip(me, step)],
             rows.at[row, core, step],
-            ep_send.at[0, step],
+            ep_send.at[0],
             ep_recv.at[0, step],
             peer(step),
         )
@@ -595,8 +599,8 @@
         return remote(
             peer_slots_ref.at[flip(near_place, step)],
             rows.at[1 - row, core, step],
-            peer_send.at[0, step],
-            peer_recv.at[0, step],
+            peer_send.at[0],
+            peer_recv.at[step],
             peer(step),
         )
 
@@ -606,23 +610,22 @@
         "cross": (1 - row, cross_send, cross_recv, core_peer),
     }
 
-    def moved_rows(step, route):
+    def moved_rows(step, route, group=0):
         origin_row, send_sem, recv_sem, device = routes_of[route]
         block = rows.at[origin_row, core, step]
         source = block
         if isinstance(step, int) and step == 0:
             source = peer_slots_ref.at[near_place] if route == "cross" else slots_ref.at[me]
-        return remote(source, block, send_sem.at[0, step], recv_sem.at[0, step], device)
+        place = 4 + step - NEAR if route == "y" else 4 + group
+        return remote(source, block, send_sem.at[0], recv_sem.at[place], device)
 
     def moved(buffer, place, route):
         origin_row, send_sem, recv_sem, device = routes_of[route]
         block = buffer.at[origin_row, core]
-        return remote(
-            block, block, send_sem.at[place, ep_count], recv_sem.at[place, ep_count], device
-        )
+        return remote(block, block, send_sem.at[2 + place], recv_sem.at[2 + place], device)
 
     info_y = remote(
-        info_ref, peer_info_ref, y_send.at[0, 0], y_recv.at[0, 0], y_peer
+        info_ref, peer_info_ref, y_send.at[1], y_recv.at[0], y_peer
     )
     for step in (6, 4, 2, 1):
         latent_ep(step).start()
@@ -693,8 +696,8 @@
     peer_own.start()
     moved_rows(0, "cross").start()
     def project():
-        for fetch in fetches[:8]:
-            fetch.wait()
+        for place, target in enumerate((query_columns_ref, latent_columns_ref)):
+            pltpu.make_async_copy(target, target, weight_sem.at[place]).wait()
         query_rows = queries[...].reshape(group_rows, queries.shape[-1])
         for side in range(2):
             projected = jnp.dot(
@@ -749,18 +752,20 @@
             own_sum[span, :] = result
             own_stats[span, :] = stats
         else:
-            sent_sum[span, :] = result
-            sent_sum[group_rows + 8 * block : group_rows + 8 * block + 8, :] = stats.T[:8]
-
-    sum_y = remote(sent_sum, far_sum, y_send.at[1, 0], y_recv.at[1, 0], y_peer)
+            sent_sum[span, :] = narrow(result)
+            sent_stats[8 * block : 8 * block + 8, :] = stats.T[:8]
+
+    sum_y = remote(sent_sum, far_sum, y_send.at[4], y_recv.at[1], y_peer)
+    stats_y = remote(sent_stats, far_stats, y_send.at[5], y_recv.at[8], y_peer)
 
     def merge():
+        stats_y.wait_recv()
         sum_y.wait_recv()
         out_lane = lax.broadcasted_iota(jnp.int32, (block_rows, head_lanes), 1)
         for block in range(2):
             span = slice(block * block_rows, (block + 1) * block_rows)
             here = own_stats[span, :]
-            there = far_sum[group_rows + 8 * block : group_rows + 8 * block + 8, :].T
+            there = far_stats[8 * block : 8 * block + 8, :].T
             result = jnp.zeros((block_rows, head_lanes), jnp.float32)
             for head in range(heads):
                 peak_here, total_here = here[:, 2 * head : 2 * head + 1], here[:, 2 * head + 1 : 2 * head + 2]
@@ -769,7 +774,7 @@
                 factor_here = jnp.exp(peak_here - peak)
                 factor_there = jnp.exp(peak_there - peak)
                 total = total_here * factor_here + total_there * factor_there
-                summed = own_sum[span, :] * factor_here + far_sum[span, :] * factor_there
+                summed = own_sum[span, :] * factor_here + wide(far_sum[span, :]) * factor_there
                 result = jnp.where(out_lane // VALUE == head, summed / total, result)
             attended[span, :] = narrow(result)
 
@@ -831,12 +836,12 @@
         step = chunks[chunk] + place
         slots_ep(step).wait_recv()
         moved_rows(step, "y").start()
-        moved_rows(step, "core").start()
+        moved_rows(step, "core", 1 + chunk).start()
 
     def arrive_far_peer(chunk, place):
         step = chunks[chunk] + place
         moved_rows(step, "y").wait_recv()
-        moved_rows(step, "cross").start()
+        moved_rows(step, "cross", 1 + chunk).start()
 
     def spans(expert):
         return slice(expert * capacity, (expert + 1) * capacity)
@@ -861,8 +866,8 @@
         return remote(
             part.at[:, 1 - core, :NEAR],
             half_rows.at[:, :NEAR],
-            half_send.at[2, 0],
-            half_recv.at[2, 0],
+            half_send.at[0],
+            half_recv.at[0],
             core_peer,
         )
 
@@ -871,8 +876,8 @@
         return remote(
             part.at[:, 1 - core, steps, spans(expert)],
             half_rows.at[:, steps, spans(expert)],
-            half_send.at[chunk, expert],
-            half_recv.at[chunk, expert],
+            half_send.at[0],
+            half_recv.at[1 + chunk * local_experts + expert],
             core_peer,
         )
 
@@ -880,8 +885,8 @@
         return remote(
             part.at[row, core, step],
             returned.at[me],
-            back_send.at[0, step],
-            back_recv.at[0, step],
+            back_send.at[0],
+            back_recv.at[0],
             peer(step),
         )
 
@@ -889,8 +894,8 @@
         return remote(
             part.at[1 - row, core, step],
             returned_peer.at[near_place],
-            peer_send.at[1, step],
-            peer_recv.at[1, step],
+            peer_send.at[1],
+            peer_recv.at[0],
             peer(step),
         )
 
@@ -898,8 +903,8 @@
         return remote(
             part.at[row, core, step, spans(expert)],
             returned.at[me, spans(expert)],
-            back_send.at[expert, step],
-            back_recv.at[expert, step],
+            back_send.at[0],
+            back_recv.at[0],
             peer(step),
         )
 
@@ -907,8 +912,8 @@
         return remote(
             part.at[1 - row, core, step, spans(expert)],
             far_rows.at[step - NEAR, spans(expert)],
-            far_send.at[expert, step],
-            far_recv.at[expert, step],
+            far_send.at[0],
+            far_recv.at[expert, step - NEAR],
             y_peer,
         )
 
@@ -950,13 +955,14 @@
             )
             back_far(step, expert).start()
 
-    def wait_rows(steps):
-        for step in steps:
-            for route in ("core", "cross"):
-                moved_rows(step, route).wait_recv()
+    def wait_rows(first, count, group):
+        for route in ("core", "cross"):
+            origin_row, send_sem, recv_sem, device = routes_of[route]
+            block = rows.at[origin_row, 1 - core, pl.ds(first, count)]
+            remote(block, block, send_sem.at[0], recv_sem.at[4 + group], device).wait_recv()
 
     def far_chunk(chunk):
-        wait_rows((chunks[chunk], chunks[chunk] + 1))
+        wait_rows(chunks[chunk], 2, 1 + chunk)
         for expert in range(local_experts):
             compute(chunks[chunk], 2, expert)
             far_half(chunk, expert).start()
@@ -969,13 +975,13 @@
     def finish_latents():
         for route in ("core", "cross"):
             moved(queries, 1, route).wait_recv()
-        for step in range(ep_count):
-            latent_core(step).wait_recv()
+        arrived = latents.at[1 - core]
+        remote(arrived, arrived, core_send.at[1], core_recv.at[1], core_peer).wait_recv()
 
     def near_compute():
         own_slots.wait()
         peer_own.wait()
-        wait_rows(range(NEAR))
+        wait_rows(0, NEAR, 0)
         for expert in range(local_experts):
             compute(0, NEAR, expert)
         near_half().start()
@@ -992,11 +998,10 @@
         project()
         attend(1, 0)
         attend(1, 1)
+        stats_y.start()
         sum_y.start()
 
-    def attend_own():
-        attend(0, 0)
-        attend(0, 1)
+    def mix_own():
         merge()
         mix()
         mixed_half.start()
@@ -1009,11 +1014,14 @@
     outer(attend_peer)
     arrive_far(0, 1)
     outer(send_far)
-    outer(attend_own)
+    outer(lambda: attend(0, 0))
+    outer(lambda: attend(0, 1))
+    outer(mix_own)
     for fetch in fetches[12:]:
         fetch.wait()
     for place in range(2):
         arrive_far_peer(0, place)
+    outer(mixed_far)
     far_chunk(0)
     for step in range(1, NEAR):
         arrive(step)
@@ -1024,17 +1032,19 @@
     inner(attend_peer)
     inner(near_compute)
     arrive_far(1, 0)
+    inner(lambda: attend(0, 0))
     arrive_far(1, 1)
+    inner(lambda: attend(0, 1))
     outer(near_compute)
     settle_far(0, 0)
     settle_far(0, 1)
+    inner(mix_own)
     settle_near()
-    inner(attend_own)
+    inner(mixed_far)
     share()
     shared_half.start()
     for place in range(2):
         arrive_far_peer(1, place)
-    mixed_far()
     far_chunk(1)
     for expert in range(local_experts):
         settle_outer(1, expert)
@@ -1042,8 +1052,8 @@
         settle_far(1, expert)
     mixed_y.wait_recv()
     both_out[0] = narrow(wide(mixed[row, core]) + wide(half_mixed[row]) + wide(far_mixed[...]))
-    for step in range(1, NEAR):
-        back_peer(step).wait_recv()
+    returns = returned_peer.at[: NEAR - 1]
+    remote(returns, returns, peer_send.at[1], peer_recv.at[0], core_peer).wait_recv()
     shared_half.wait_recv()
     for start in range(0, width, stripe):
         cut = slice(start, start + stripe)
@@ -1056,11 +1066,8 @@
             + wide(half_shared[1 - row, :, cut])
         )
     shared_y.start()
-    for step in range(1, NEAR):
-        back_near(step).wait_recv()
-    for step in far_steps:
-        for expert in range(local_experts):
-            back_far(step, expert).wait_recv()
+    returns = returned.at[: ep_count - 1]
+    remote(returns, returns, back_send.at[0], back_recv.at[0], core_peer).wait_recv()
     shared_y.wait_recv()
     for start in range(0, width, stripe):
         cut = slice(start, start + stripe)
@@ -1073,29 +1080,25 @@
             + wide(far_shared[:, cut])
         )
 
-    for step in range(1, ep_count):
-        latent_ep(step).wait_send()
-        slots_ep(step).wait_send()
-    for step in range(ep_count):
-        latent_core(step).wait_send()
-        for route in ("core", "cross"):
-            moved_rows(step, route).wait_send()
-    for step in range(1, NEAR):
-        peer_slots_ep(step).wait_send()
-        back_near(step).wait_send()
-        back_peer(step).wait_send()
-    for step in far_steps:
-        moved_rows(step, "y").wait_send()
-        for expert in range(local_experts):
-            back_far(step, expert).wait_send()
-            y_copy(step, expert).wait_send()
+    blocks = rows.at[0, 0]
+    for source, sem in (
+        (slots_ref.at[: ep_count - 1], ep_send.at[0]),
+        (latents.at[0, : ep_count - 1], ep_send.at[1]),
+        (blocks, core_send.at[0]),
+        (latents.at[0], core_send.at[1]),
+        (blocks, cross_send.at[0]),
+        (rows.at[0, 0, NEAR:], y_send.at[0]),
+        (rows.at[0, 0, : NEAR - 1], peer_send.at[0]),
+        (rows.at[0, 0, : NEAR - 1], peer_send.at[1]),
+        (rows.at[0, 0, : ep_count - 1], back_send.at[0]),
+        (rows.at[0, 0, NEAR:], far_send.at[0]),
+        (part.at[0], half_send.at[0]),
+    ):
+        remote(source, source, sem, core_recv.at[0], core_peer).wait_send()
     for route in ("y", "core", "cross"):
         moved(queries, 1, route).wait_send()
         moved(tokens, 0, route).wait_send()
-    for chunk in range(2):
-        for expert in range(local_experts):
-            far_half(chunk, expert).wait_send()
-    for copy in (info_y, sum_y, near_half(), shared_half, mixed_half, shared_y, mixed_y):
+    for copy in (info_y, sum_y, stats_y, shared_half, mixed_half, shared_y, mixed_y):
         copy.wait_send()
 
 
@@ -1163,15 +1166,34 @@
             precise(8, 128),
             precise(group_rows, head_lanes),
             precise(group_rows, head_lanes),
-            precise(group_rows + 16, head_lanes),
-            precise(group_rows + 16, head_lanes),
+            held(group_rows, head_lanes),
+            held(group_rows, head_lanes),
+            precise(16, head_lanes),
+            precise(16, head_lanes),
         ]
-        + [sems(2, ep_count + 1)] * 8
-        + [sems(2, NEAR)] * 2
-        + [sems(local_experts, ep_count)] * 4
-        + [sems(3, local_experts)] * 2
-        + [sems(4)] * 2
-        + [sems(2), sems(15), sems(10)],
+        + [
+            sems(2),
+            sems(2, ep_count),
+            sems(6),
+            sems(9),
+            sems(4),
+            sems(7),
+            sems(4),
+            sems(7),
+            sems(2),
+            sems(NEAR),
+            sems(1),
+            sems(1),
+            sems(1),
+            sems(local_experts, ep_count - NEAR),
+            sems(1),
+            sems(1 + 2 * local_experts),
+            sems(4),
+            sems(4),
+            sems(2),
+            sems(9),
+            sems(10),
+        ],
         compiler_params=pltpu.CompilerParams(
             collective_id=0, has_side_effects=True, vmem_limit_bytes=VMEM_LIMIT
         ),

time: 74.6 us -> 72.3 us (0.969)
  Pallas kernels: 71.9 us -> 69.6 us
    pallas_call x1, Pallas kernels: 71.9 us -> 69.6 us  [block_call(): pl.pallas_call(lambda *refs: block_kernel(ep_count, capacity, *refs), out...]
where the time goes in v4:
time: 72.3 us; the launch traced here: 72.1 us
  Pallas kernels  69.6 us (96%)
  local copies, waits for them, and re-layouts  1.87 us (3%)
    pallas_call x1, Pallas kernels, block_call(): pl.pallas_call(lambda *refs: block_kernel(ep_count, capacity, *refs), out...  69.6 us
    squeeze x1, local copies, waits for them, and re-layouts, shards(): return (both[0], both[1])  1.87 us

profile of v4, /device:TPU:0, one launch (start us, length us, event | category | flops | bytes accessed | tf_op | source)
XLA Modules:
  0.0 72.1 jit_solution(571023151949364013)
XLA Ops:
  0.6 69.6 %block.1 = bf16[2,64,2048]{2,1,0:T(8,128)(2,1)} custom-call(bf16[64,512]{1,0:T(8,128)(2,1)} %refs_0_.1, bf16[64,256]{1,0:T(8,128)(2,1)} %refs_1_.1, bf16[32,64]{1,0:T(8,128)(2,1)} %bitcast.10, f32[1,512]{1,0:T(1,128)} %bitcast.12, f32[1,256]{1,0:T(1,128)} %bitcast.13, bf16[64,2048]{1,0:T(8,128)(2,1)} %refs_5_.1, f32[1,2048]{1,0:T(1,128)} %bitcast.11, ...), custom_call_target="tpu_custom_call" | custom-call | tf_op jit(solution)/shard_map/block/pallas_call | solution.py:1127
  70.3 1.9 %slice_bitcast_fusion = (bf16[64,2048]{1,0:T(8,128)(2,1)}, bf16[64,2048]{1,0:T(8,128)(2,1)}) fusion(bf16[2,64,2048]{2,1,0:T(8,128)(2,1)} %block.1), kind=kLoop, calls=%fused_computation | loop fusion | bytes 1048576 | tf_op jit(solution)/shard_map/squeeze | solution.py:1282
